TPU v7x, 256 devices: a whole 4x4x8 slice. The times are simulated.
256 devices in a mesh: sp: 64 (over z, x, core), tp: 4 (over y).
Axes of the slice: x: 4, y: 4, z: 8, core: 2. Of those that a mesh axis runs over, the one named last changes fastest.
Arguments:
- residual: bfloat16 [24576, 2048], P(('sp', 'tp')), may hold values from -6 to 6
- queries: bfloat16 [24576, 1024], P('sp', 'tp'), may hold values from -2.5 to 2.5
- keys: bfloat16 [24576, 256], P('sp', 'tp'), may hold values from -2.5 to 2.5
- values: bfloat16 [24576, 256], P('sp', 'tp'), may hold values from -6 to 6
- documents: int32 [24576], P('sp'), may hold values from 0 to 32, never falling along the last dimension, each value on 1 to 1536 neighbouring positions
- sink: float32 [16], P('tp'), may hold values from 3 to 7
- out_weight: bfloat16 [1024, 2048], replicated, may hold values from -0.1875 to 0.1875
- mix_gain: float32 [2048], replicated, may hold values from 0.1 to 1.9
- ffn_gain: float32 [2048], replicated, may hold values from 0.1 to 1.9
- out_gain: float32 [2048], replicated, may hold values from 0.1 to 1.9
- routes: int32 [24576, 4], P(('sp', 'tp')), may hold values from 0 to 63, all different within a row; in each aligned block of 96 rows (0 to 95, 96 to 191, ...) at most 8 rows name the same one
- route_logits: float32 [24576, 4], P(('sp', 'tp')), may hold values from -4 to 4
- gate_weight: bfloat16 [64, 2048, 2048], P('sp', None, 'tp'), may hold values from -1.41421356 to 1.41421356
- up_weight: bfloat16 [64, 2048, 2048], P('sp', None, 'tp'), may hold values from -1.41421356 to 1.41421356
- down_weight: bfloat16 [64, 2048, 2048], P('sp', 'tp'), may hold values from -0.125 to 0.125
Outputs:
- mixed: bfloat16 [24576, 2048], P(('sp', 'tp'))
Inputs may be any that keep to these rules, and one draw needn't show every extreme that they name: `routes`: each row names 4 different experts. In each aligned block of rows held by one device, no expert is named by more than 8 rows, a bound that some block reaches. `documents`: document numbers never fall along the positions; each document has 1 to 1536 positions, and one has exactly 1536.
All inputs are finite; a program needn't handle non-finite values.
Results may differ from a plain program's by a relative error of at most 0.017.
Values may be sent and summed in bfloat16 or wider, within the bound.
A program may use at most 128 MiB of HBM per device.

v0:
```python
import jax
import jax.numpy as jnp
from jax import lax
from jax.experimental import pallas as pl
from jax.experimental.pallas import tpu as pltpu
from jax.sharding import PartitionSpec as P

HD = 64
TOPK = 4
W = 128
D = 2048
CAP = 8
NZ, NX, NT = 8, 4, 4
NCOL = NZ * NX
MESH = pl.DeviceIdType.MESH


NEAR_Z = (1, 7, 2, 6, 3, 5)
OFFSETS = (
    tuple((0, dx) for dx in (1, 3, 2, 0))
    + tuple((dz, dx) for dx in (1, 3) for dz in NEAR_Z)
    + tuple((4, dx) for dx in (1, 3, 2, 0))
    + tuple((dz, dx) for dx in (2, 0) for dz in NEAR_Z)
)
SELF = OFFSETS.index((0, 0))
GROUP = 4
GROUPS = NCOL // GROUP
BACK = (4, 1, 2, 3, 5, 6, 7, 0)
HALF = 512
TILE = 256


def place():
    s = lax.axis_index("sp")
    t = lax.axis_index("tp")
    core = lax.rem(s, 2)
    column = lax.div(s, 2)
    return s, t, core, lax.div(column, NX), lax.rem(column, NX)


def shifted(z, x, core, dz, dx):
    return (lax.rem(z + dz, NZ) * NX + lax.rem(x + dx, NX)) * 2 + core


def greet(partners):
    barrier = pltpu.get_barrier_semaphore()
    for partner in partners:
        pl.semaphore_signal(barrier, inc=1, device_id=partner, device_id_type=MESH)
    pl.semaphore_wait(barrier, len(partners))


def partners_of(s, t, core, z, x):
    found = [(s, t + 1 - 2 * lax.rem(t, 2))]
    for index, (dz, dx) in enumerate(OFFSETS):
        column = shifted(z, x, core, dz, dx)
        found.append((column, 3 - t))
        if index != SELF:
            found.append((column, t))
    return found


def dispatch_kernel(out_ref, in_ref, send_sem, recv_sem, own_sem, far_send_sem):
    s, t, core, z, x = place()
    pair = (s, t + 1 - 2 * lax.rem(t, 2))
    greet(partners_of(s, t, core, z, x))
    own = pltpu.make_async_copy(out_ref.at[0, SELF], in_ref.at[0, SELF], own_sem)
    own.start()
    sends = []
    for index, (dz, dx) in enumerate(OFFSETS):
        column = shifted(z, x, core, dz, dx)
        for kind in range(2):
            if kind == 0 and index == SELF:
                continue
            copy = pltpu.make_async_remote_copy(
                src_ref=out_ref.at[kind, index],
                dst_ref=in_ref.at[kind, index],
                send_sem=send_sem.at[kind, index],
                recv_sem=recv_sem.at[kind, index],
                device_id=(column, t if kind == 0 else 3 - t),
                device_id_type=MESH,
            )
            copy.start()
            sends.append(copy)
    arrived = {}
    for copy, key in zip(sends, [(k, i) for i in range(NCOL) for k in range(2) if (k, i) != (0, SELF)]):
        arrived[key] = copy
    forwards = []
    for group in range(GROUPS):
        for kind in range(2):
            for index in range(group * GROUP, (group + 1) * GROUP):
                if (kind, index) == (0, SELF):
                    own.wait()
                else:
                    arrived[kind, index].wait_recv()
            block = pl.ds(group * GROUP, GROUP)
            copy = pltpu.make_async_remote_copy(
                src_ref=in_ref.at[kind, block],
                dst_ref=in_ref.at[2 + kind, block],
                send_sem=far_send_sem.at[0, kind, group],
                recv_sem=far_send_sem.at[1, kind, group],
                device_id=pair,
                device_id_type=MESH,
            )
            copy.start()
            forwards.append(copy)
    for copy in sends:
        copy.wait_send()
    for copy in forwards:
        copy.wait()


def dispatch(outgoing):
    return pl.pallas_call(
        dispatch_kernel,
        out_shape=jax.ShapeDtypeStruct((4, NCOL, CAP, D), jnp.bfloat16),
        in_specs=[pl.BlockSpec(memory_space=pltpu.VMEM)],
        out_specs=pl.BlockSpec(memory_space=pl.ANY),
        scratch_shapes=[
            pltpu.SemaphoreType.DMA((2, NCOL)),
            pltpu.SemaphoreType.DMA((2, NCOL)),
            pltpu.SemaphoreType.DMA,
            pltpu.SemaphoreType.DMA((2, 2, GROUPS)),
        ],
        compiler_params=pltpu.CompilerParams(
            collective_id=0, has_side_effects=True, vmem_limit_bytes=16 << 20
        ),
        cost_estimate=pl.CostEstimate(flops=0, bytes_accessed=150_000_000, transcendentals=0),
    )(outgoing)


def expert_kernel(
    rows_ref,
    gate_one,
    gate_two,
    up_one,
    up_two,
    down_one,
    down_two,
    ret_ref,
    block_rows,
    hidden,
    mine,
    away,
    theirs,
    total,
    pair_sem,
    send_sem,
    recv_sem,
):
    s, t, core, z, x = place()
    pair = (s, t + 1 - 2 * lax.rem(t, 2))
    greet(partners_of(s, t, core, z, x))
    count = 4 * GROUP * CAP
    pairs = {}
    sends = []
    own = []

    def activate(gate, up, target, column):
        columns = pl.ds(pl.multiple_of(column * TILE, TILE), TILE)
        gate_pre = jnp.dot(block_rows[...], gate[:, columns], preferred_element_type=jnp.float32)
        up_pre = jnp.dot(block_rows[...], up[:, columns], preferred_element_type=jnp.float32)
        gated = jnp.minimum(gate_pre, 7.0)
        upper = jnp.clip(up_pre, -7.0, 7.0)
        value = (upper + 1.0) * gated * jax.nn.sigmoid(1.702 * gated)
        columns = pl.ds(pl.multiple_of(target * HALF + column * TILE, TILE), TILE)
        hidden[:, columns] = value.astype(jnp.bfloat16)

    def compute(group):
        block = pl.ds(group * GROUP, GROUP)
        block_rows[...] = (
            rows_ref[:, block].astype(jnp.float32).reshape(count, D).astype(jnp.bfloat16)
        )

        @pl.loop(0, HALF // TILE)
        def _(column):
            activate(gate_one, up_one, 0, column)
            activate(gate_two, up_two, 1, column)

        @pl.loop(0, D // TILE)
        def _(column):
            columns = pl.ds(pl.multiple_of(column * TILE, TILE), TILE)
            term = jnp.dot(
                hidden[:, :HALF], down_one[:, columns], preferred_element_type=jnp.float32
            ) + jnp.dot(hidden[:, HALF:], down_two[:, columns], preferred_element_type=jnp.float32)
            term = term.reshape(4, GROUP, CAP, TILE).astype(jnp.bfloat16)
            mine[:, block, :, columns] = term[:2]
            away[:, block, :, columns] = term[2:]

    def swap(group):
        block = pl.ds(group * GROUP, GROUP)
        for kind in (1, 0):
            copy = pltpu.make_async_remote_copy(
                src_ref=away.at[kind, block],
                dst_ref=theirs.at[kind, block],
                send_sem=pair_sem.at[0, kind, group],
                recv_sem=pair_sem.at[1, kind, group],
                device_id=pair,
                device_id_type=MESH,
            )
            copy.start()
            pairs[kind, group] = copy

    def add(group):
        block = pl.ds(group * GROUP, GROUP)
        for kind in (1, 0):
            pairs[kind, group].wait_recv()
            total[kind, block] = (
                mine[kind, block].astype(jnp.float32) + theirs[kind, block].astype(jnp.float32)
            ).astype(jnp.bfloat16)

    def home(group):
        for kind in (1, 0):
            for index in range(group * GROUP, (group + 1) * GROUP):
                dz, dx = OFFSETS[index]
                if (kind, index) == (0, SELF):
                    copy = pltpu.make_async_copy(
                        total.at[kind, index], ret_ref.at[kind, index], send_sem.at[kind, index]
                    )
                    own.append(copy)
                else:
                    column = shifted(z, x, core, NZ - dz, NX - dx)
                    copy = pltpu.make_async_remote_copy(
                        src_ref=total.at[kind, index],
                        dst_ref=ret_ref.at[kind, index],
                        send_sem=send_sem.at[kind, index],
                        recv_sem=recv_sem.at[kind, index],
                        device_id=(column, t if kind == 0 else 3 - t),
                        device_id_type=MESH,
                    )
                    sends.append(copy)
                copy.start()

    behind = 2
    for step in range(GROUPS + behind):
        if step < GROUPS:
            compute(BACK[step])
        if step >= behind:
            add(BACK[step - behind])
        if step < GROUPS:
            swap(BACK[step])
        if step >= behind:
            home(BACK[step - behind])
    for copy in pairs.values():
        copy.wait_send()
    for copy in own:
        copy.wait()
    for copy in sends:
        copy.wait()


def expert_outputs(rows_in, halves):
    half = (2, NCOL, CAP, D)
    flat = [one for pair in halves for one in pair]
    vmem = pl.BlockSpec(memory_space=pltpu.VMEM)
    return pl.pallas_call(
        expert_kernel,
        out_shape=jax.ShapeDtypeStruct(half, jnp.bfloat16),
        in_specs=[vmem] * 7,
        out_specs=pl.BlockSpec(memory_space=pl.ANY),
        scratch_shapes=[
            pltpu.VMEM((4 * GROUP * CAP, D), jnp.bfloat16),
            pltpu.VMEM((4 * GROUP * CAP, 2 * HALF), jnp.bfloat16),
            pltpu.VMEM(half, jnp.bfloat16),
            pltpu.VMEM(half, jnp.bfloat16),
            pltpu.VMEM(half, jnp.bfloat16),
            pltpu.VMEM(half, jnp.bfloat16),
            pltpu.SemaphoreType.DMA((2, 2, GROUPS)),
            pltpu.SemaphoreType.DMA((2, NCOL)),
            pltpu.SemaphoreType.DMA((2, NCOL)),
        ],
        compiler_params=pltpu.CompilerParams(
            collective_id=1, has_side_effects=True, vmem_limit_bytes=40 << 20
        ),
        cost_estimate=pl.CostEstimate(
            flops=13_000_000_000, bytes_accessed=150_000_000, transcendentals=0
        ),
    )(rows_in, *flat)


def weight_moves(sp_count):
    first, second = [], []
    for s in range(sp_count):
        for t in range(NT):
            core, side = s % 2, t // 2
            sibling = (s ^ 1) * NT + t
            second.append((s * NT + t, sibling))
            first.append((s * NT + t, sibling if core == side else s * NT + 3 - t))
    return first, second


def extended(block, sides, width):
    for axis, dim in sides:
        count = lax.axis_size(axis)
        forward = [(i, i + 1) for i in range(count - 1)]
        backward = [(target, source) for source, target in forward]
        low = lax.ppermute(
            lax.slice_in_dim(block, block.shape[dim] - width, None, axis=dim), axis, forward
        )
        high = lax.ppermute(lax.slice_in_dim(block, 0, width, axis=dim), axis, backward)
        block = jnp.concatenate([low, block, high], axis=dim)
    return block


def turn_heads(block, positions, head_count):
    total = block.shape[0]
    heads = block.astype(jnp.float32).reshape(total, head_count, HD)
    half_size = HD // 2
    inverse = 10000.0 ** (-jnp.arange(half_size, dtype=jnp.float32) / half_size)
    angles = positions.astype(jnp.float32)[:, None] * inverse[None, :]
    cosine = jnp.cos(angles)[:, None, :]
    sine = jnp.sin(angles)[:, None, :]
    first_half = heads[..., :half_size]
    second_half = heads[..., half_size:]
    turned = jnp.concatenate(
        [first_half * cosine - second_half * sine, second_half * cosine + first_half * sine],
        axis=-1,
    )
    return turned.reshape(total, head_count * HD).astype(jnp.bfloat16)


def rms_scale(vector):
    return vector * lax.rsqrt(jnp.mean(vector * vector, axis=-1, keepdims=True) + 1e-06)


def windows(padded_rows, blocks):
    tiled = padded_rows.reshape((blocks + 2, W) + padded_rows.shape[1:])
    return jnp.concatenate([tiled[:-2], tiled[1:-1], tiled[2:]], axis=1)


def slots(route_rows, expert_count):
    flat_routes = route_rows.reshape(route_rows.shape[0] * TOPK)
    onehot_hits = (
        flat_routes[:, None] == jnp.arange(expert_count, dtype=jnp.int32)[None, :]
    ).astype(jnp.int32)
    slot_number = jnp.sum(jnp.cumsum(onehot_hits, axis=0) * onehot_hits, axis=1) - 1
    _, t, _, z, x = place()
    column = flat_routes // 2
    dz = (column // NX - z + NZ) % NZ
    dx = (column % NX - x + NX) % NX
    rank = jnp.zeros_like(dz)
    for index, (far_z, far_x) in enumerate(OFFSETS):
        rank = jnp.where((dz == far_z) & (dx == far_x), index, rank)
    kind = jnp.where(flat_routes % 2 == t // 2, 0, 1)
    position = (kind * NCOL + rank) * CAP + slot_number
    return position.reshape(route_rows.shape)


def body(
    residual,
    queries,
    keys,
    values,
    documents,
    sink,
    out_weight,
    mix_gain,
    ffn_gain,
    out_gain,
    routes,
    route_logits,
    gate_weight,
    up_weight,
    down_weight,
):
    tok_rows = queries.shape[0]
    head_count = queries.shape[1] // HD
    kv_count = keys.shape[1] // HD
    group_size = head_count // kv_count
    sp_count = lax.axis_size("sp")
    first, second = weight_moves(sp_count)
    gate_one = lax.ppermute(gate_weight[0], ("sp", "tp"), first)
    offset = lax.axis_index("sp") * tok_rows
    positions = offset + jnp.arange(tok_rows, dtype=jnp.int32)
    q_turned = turn_heads(queries, positions, head_count)
    k_turned = turn_heads(keys, positions, kv_count)
    paired = jnp.concatenate([k_turned, values], axis=1)
    wide_pairs, wide_docs = (
        extended(paired, (("sp", 0),), W),
        extended(documents, (("sp", 0),), W),
    )
    blocks = tok_rows // W
    query_blocks = q_turned.reshape(blocks, W, kv_count, group_size, HD)
    pair_win = windows(wide_pairs, blocks)
    key_win = pair_win[..., : kv_count * HD].reshape(blocks, 3 * W, kv_count, HD)
    value_win = pair_win[..., kv_count * HD :].reshape(blocks, 3 * W, kv_count, HD)
    doc_win = windows(wide_docs, blocks)
    doc_query = documents.reshape(blocks, W)
    block_ids = jnp.arange(blocks, dtype=jnp.int32)[:, None, None]
    query_pos = offset + block_ids * W + jnp.arange(W, dtype=jnp.int32)[None, :, None]
    key_pos = offset + (block_ids - 1) * W + jnp.arange(3 * W, dtype=jnp.int32)[None, None, :]
    keep_mask = (
        (jnp.abs(query_pos - key_pos) <= W) & (key_pos >= 0) & (key_pos < tok_rows * sp_count)
    )
    keep_mask = keep_mask & (doc_query[:, :, None] == doc_win[:, None, :])
    scores = jnp.einsum(
        "nqhgd,nkhd->nhgqk", query_blocks, key_win, preferred_element_type=jnp.float32
    ) * HD ** (-0.5)
    exponent = jnp.where(keep_mask[:, None, None], jnp.exp(scores), 0.0)
    denominator = jnp.sum(exponent, axis=-1, keepdims=True) + jnp.exp(sink).reshape(
        1, kv_count, group_size, 1, 1
    )
    probs = (exponent / denominator).astype(jnp.bfloat16)
    attended = jnp.einsum("nhgqk,nkhd->nqhgd", probs, value_win, preferred_element_type=jnp.float32)
    attended = attended.astype(jnp.bfloat16).reshape(tok_rows, head_count * HD)
    all_heads = lax.all_to_all(attended, "tp", split_axis=0, concat_axis=1, tiled=True)
    all_heads, up_weight, down_weight = lax.optimization_barrier(
        (all_heads, up_weight, down_weight)
    )
    up_one = lax.ppermute(up_weight[0], ("sp", "tp"), first)
    down_one = lax.ppermute(down_weight[0], ("sp", "tp"), first)
    gate_two = lax.ppermute(gate_one, ("sp", "tp"), second)
    projected = jnp.dot(all_heads, out_weight, preferred_element_type=jnp.float32)
    after_mix = residual.astype(jnp.float32) + rms_scale(projected) * mix_gain
    normed = (rms_scale(after_mix) * ffn_gain).astype(jnp.bfloat16)
    expert_count = gate_weight.shape[0] * sp_count
    position = slots(routes, expert_count)
    hits = position[:, :, None] == jnp.arange(expert_count * CAP, dtype=jnp.int32)
    picks = jnp.any(hits, axis=1).astype(jnp.bfloat16)
    outgoing = lax.dot_general(
        picks, normed, (((0,), (0,)), ((), ())), preferred_element_type=jnp.float32
    ).astype(jnp.bfloat16)
    rows_in = dispatch(outgoing.reshape(2, NCOL, CAP, D))
    up_two = lax.ppermute(up_one, ("sp", "tp"), second)
    down_two = lax.ppermute(down_one, ("sp", "tp"), second)
    halves = ((gate_one, gate_two), (up_one, up_two), (down_one, down_two))
    returned = expert_outputs(rows_in, halves)
    returned = returned.reshape(expert_count * CAP, D)
    exp_logits = jnp.exp(route_logits)
    route_weights = exp_logits / jnp.sum(exp_logits, axis=-1, keepdims=True)
    spread = jnp.sum(jnp.where(hits, route_weights[:, :, None], 0.0), axis=1)
    coarse = lax.reduce_precision(spread, 8, 7)
    expert_mix = jnp.dot(
        coarse.astype(jnp.bfloat16), returned, preferred_element_type=jnp.float32
    ) + jnp.dot(
        (spread - coarse).astype(jnp.bfloat16), returned, preferred_element_type=jnp.float32
    )
    return (after_mix + rms_scale(expert_mix) * out_gain).astype(jnp.bfloat16)


def solution(mesh):
    in_specs = (
        P(("sp", "tp"), None),
        P("sp", "tp"),
        P("sp", "tp"),
        P("sp", "tp"),
        P("sp"),
        P("tp"),
        P(),
        P(),
        P(),
        P(),
        P(("sp", "tp"), None),
        P(("sp", "tp"), None),
        P("sp", None, "tp"),
        P("sp", None, "tp"),
        P("sp", "tp", None),
    )
    out_specs = P(("sp", "tp"), None)

    return jax.shard_map(body, mesh=mesh, in_specs=in_specs, out_specs=out_specs, check_vma=False)
```

profile of v0, /device:TPU:1, one launch (start us, length us, event | category | flops | bytes accessed | tf_op | source)
XLA Modules:
  0.0 254.1 jit_solution(16078845123880483865)
XLA Ops:
  0.0 0.8 bitcast_convert_fusion
  0.9 0.3 fusion.29
  1.1 0.7 fusion.32
  1.9 4.5 %collective-permute-start = (bf16[128,128]{0,1:T(8,128)(2,1)S(1)}, bf16[128,128]{0,1:T(8,128)(2,1)S(1)}, u32[]{:S(2)}, u32[]{:S(2)}) collective-permute-start(bf16[128,128]{0,1:T(8,128)(2,1)S(1)} %get-tuple-element.18), channel_id=1, source_target_pairs={{0,4},{4,8},{8,12},{12,16},{16,20},{20,24},{24,28},{28,32},{32,36}... | collective-permute-start | bytes 98312 | tf_op jit(solution)/shard_map/ppermute | solution.py:296
  6.4 1.9 collective-permute-start.1
  8.3 0.8 fusion.48
  9.1 3.6 %collective-permute-start.2 = (s32[128]{0:T(128)S(1)}, s32[128]{0:T(128)S(1)}, u32[]{:S(2)}, u32[]{:S(2)}) collective-permute-start(s32[128]{0:T(128)S(1)} %get-tuple-element.24), channel_id=1, source_target_pairs={{0,4},{4,8},{8,12},{12,16},{16,20},{20,24},{24,28},{28,32},{32,36}... | collective-permute-start | bytes 1544 | tf_op jit(solution)/shard_map/ppermute | solution.py:296
  12.7 1.9 collective-permute-start.3
  14.7 0.1 fusion.35
  14.7 0.1 iota_add_fusion
  14.8 0.3 multiply_cosine_fusion
  15.1 1.1 copy.90
  16.2 0.1 subtract_convert_fusion
  16.3 0.1 iota_add_fusion.1
  16.3 1.3 collective-permute-done.3
  17.6 0.9 fusion.12
  18.6 0.1 copy.84
  18.7 0.1 copy.87
  18.8 0.1 copy.85
  19.0 0.1 copy.88
  19.1 0.1 copy.86
  19.2 0.1 copy.89
  19.4 0.7 fusion
  20.1 0.1 broadcast_add_fusion
  20.2 0.7 fusion.6
  20.9 0.3 copy.103
  21.1 1.0 reshape.524
  22.1 4.2 %all-to-all-start = ((bf16[4,96,256]{2,1,0:T(8,128)(2,1)}), bf16[4,96,256]{2,1,0:T(8,128)(2,1)S(1)}, u32[]{:S(2)}, u32[]{:S(2)}) async-start(bf16[4,96,256]{2,1,0:T(8,128)(2,1)} %reshape.524), calls=%async_computation | async-start | bytes 393216 | tf_op jit(solution)/shard_map/all_to_all | solution.py:405
  26.3 2.7 %collective-permute-start.4 = (bf16[2048,512]{1,0:T(8,128)(2,1)}, bf16[2048,512]{1,0:T(8,128)(2,1)S(1)}, u32[]{:S(2)}, u32[]{:S(2)}) collective-permute-start(bf16[2048,512]{1,0:T(8,128)(2,1)} %bitcast.105), channel_id=1, source_target_pairs={{0,4},{1,5},{2,1},{3,0},{4,7},{5,6},{6,2},{7,3},{8,12},{9,13},{10,... | collective-permute-start | bytes 6291464 | tf_op jit(solution)/shard_map/ppermute | solution.py:371
  28.9 3.4 %all-to-all-done = bf16[4,96,256]{2,1,0:T(8,128)(2,1)S(1)} async-done(((bf16[4,96,256]{2,1,0:T(8,128)(2,1)}), bf16[4,96,256]{2,1,0:T(8,128)(2,1)S(1)}, u32[]{:S(2)}, u32[]{:S(2)}) %all-to-all-start) | async-done | bytes 196640 | tf_op jit(solution)/shard_map/all_to_all | solution.py:405
  32.3 0.1 collective-permute-start.6
  32.5 0.1 collective-permute-start.8
  32.6 0.1 copy.96
  32.7 0.1 eq.204
  32.8 0.1 eq.200
  32.9 0.9 reduce-window.6
  33.8 0.2 slice_reduce_fusion
  34.1 0.1 fusion.22
  34.2 0.1 sub.78
  34.4 0.1 copy.99
  34.4 17.8 %collective-permute-done.4.gate_one = bf16[2048,512]{1,0:T(8,128)(2,1)S(1)} collective-permute-done((bf16[2048,512]{1,0:T(8,128)(2,1)}, bf16[2048,512]{1,0:T(8,128)(2,1)S(1)}, u32[]{:S(2)}, u32[]{:S(2)}) %collective-permute-start.4) | collective-permute-done | bytes 2097184 | tf_op jit(solution)/shard_map/ppermute | solution.py:371
  52.2 2.0 collective-permute-start.5
  54.3 20.4 %collective-permute-done.6.up_one = bf16[2048,512]{1,0:T(8,128)(2,1)} collective-permute-done((bf16[2048,512]{1,0:T(8,128)(2,1)}, bf16[2048,512]{1,0:T(8,128)(2,1)}, u32[]{:S(2)}, u32[]{:S(2)}) %collective-permute-start.6) | collective-permute-done | bytes 2097184 | tf_op jit(solution)/shard_map/ppermute | solution.py:409
  74.7 2.2 collective-permute-start.7
  76.9 20.3 %collective-permute-done.8.down_one = bf16[512,2048]{1,0:T(8,128)(2,1)} collective-permute-done((bf16[512,2048]{1,0:T(8,128)(2,1)}, bf16[512,2048]{1,0:T(8,128)(2,1)}, u32[]{:S(2)}, u32[]{:S(2)}) %collective-permute-start.8) | collective-permute-done | bytes 2097184 | tf_op jit(solution)/shard_map/ppermute | solution.py:410
  97.2 2.2 collective-permute-start.9
  99.4 0.1 multiply_add_fusion.1
  99.4 0.2 fusion.9
  99.6 0.2 select_reduce_fusion
  99.8 0.0 copy-start.1
  99.8 0.0 copy-start.3
  99.8 0.0 copy-start.5
  99.8 3.1 %multiply_reduce_fusion.2 = (f32[96]{0:T(128)S(1)}, f32[96,2048]{1,0:T(8,128)S(1)}) fusion(bf16[96,1024]{1,0:T(8,128)(2,1)S(1)} %bitcast.98, bf16[1024,2048]{1,0:T(8,128)(2,1)} %param.21), kind=kOutput, calls=%fused_computation.17 | convolution fusion | flops 403046304 | bytes 5177728 | tf_op jit(solution)/shard_map/dot_general | solution.py:412
  103.0 0.3 multiply_reduce_fusion.1
  103.3 0.8 convolution_convert_fusion
  104.2 74.8 %shard_map.145.rows_ref = bf16[4,32,8,2048]{3,2,1,0:T(8,128)(2,1)S(1)} custom-call(bf16[2,32,8,2048]{3,2,1,0:T(8,128)(2,1)S(1)} %bitcast.93), custom_call_target="tpu_custom_call" | custom-call | bytes 150000000 | tf_op jit(solution)/shard_map/pallas_call | solution.py:113
  179.0 1.9 copy-done
  181.0 1.3 copy-done.9
  182.3 69.5 %shard_map.146 = bf16[2,32,8,2048]{3,2,1,0:T(8,128)(2,1)S(1)} custom-call(bf16[4,32,8,2048]{3,2,1,0:T(8,128)(2,1)} %copy-done, bf16[2048,512]{1,0:T(8,128)(2,1)S(1)} %collective-permute-done.4.gate_one, bf16[2048,512]{1,0:T(8,128)(2,1)S(1)} %collective-permute-done.5.gate_two, bf16[2048,512]{1,0:T(8,128)(2,1)} %collective-permute-done.6.up_one, ...), custom_call_target="tpu_custom_call" | custom-call | flops 12999999488 | bytes 150000000 | tf_op jit(solution)/shard_map/pallas_call | solution.py:255
  251.8 0.5 fusion.19
  252.3 0.0 copy-start.6
  252.3 0.6 multiply_reduce_fusion
  252.9 0.1 copy-done.6
  253.0 1.1 add_convert_fusion
  (41 shorter events, 0.3 us)
Async XLA Ops:
  0.0 18.5 %copy-start.2 = (bf16[384,64]{0,1:T(8,128)(2,1)S(1)}, bf16[384,64]{0,1:T(8,128)(2,1)}, u32[]{:S(2)}) copy-start(bf16[384,64]{0,1:T(8,128)(2,1)} %param.18) | copy-start | bytes 147460
  0.0 17.6 %copy-start.4 = (s32[384]{0:T(512)S(1)}, s32[384]{0:T(512)}, u32[]{:S(2)}) copy-start(s32[384]{0:T(512)} %param.19) | copy-start | bytes 4612
  0.0 16.3 %copy-start.10 = (f32[4]{0:T(128)S(1)}, f32[4]{0:T(128)}, u32[]{:S(2)}) copy-start(f32[4]{0:T(128)} %param.20) | copy-start | bytes 52
  1.9 16.6 %collective-permute-start = (bf16[128,128]{0,1:T(8,128)(2,1)S(1)}, bf16[128,128]{0,1:T(8,128)(2,1)S(1)}, u32[]{:S(2)}, u32[]{:S(2)}) collective-permute-start(bf16[128,128]{0,1:T(8,128)(2,1)S(1)} %get-tuple-element.18), channel_id=1, source_target_pairs={{0,4},{4,8},{8,12},{12,16},{16,20},{20,24},{24,28},{28,32},{32,36}... | collective-permute-start | bytes 98312 | tf_op jit(solution)/shard_map/ppermute | solution.py:296
  6.4 12.1 %collective-permute-start.1 = (bf16[128,128]{0,1:T(8,128)(2,1)S(1)}, bf16[128,128]{0,1:T(8,128)(2,1)S(1)}, u32[]{:S(2)}, u32[]{:S(2)}) collective-permute-start(bf16[128,128]{0,1:T(8,128)(2,1)S(1)} %get-tuple-element.19), channel_id=1, source_target_pairs={{4,0},{8,4},{12,8},{16,12},{20,16},{24,20},{28,24},{32,28},{36,32}... | collective-permute-start | bytes 98312 | tf_op jit(solution)/shard_map/ppermute | solution.py:299
  9.1 7.3 %collective-permute-start.2 = (s32[128]{0:T(128)S(1)}, s32[128]{0:T(128)S(1)}, u32[]{:S(2)}, u32[]{:S(2)}) collective-permute-start(s32[128]{0:T(128)S(1)} %get-tuple-element.24), channel_id=1, source_target_pairs={{0,4},{4,8},{8,12},{12,16},{16,20},{20,24},{24,28},{28,32},{32,36}... | collective-permute-start | bytes 1544 | tf_op jit(solution)/shard_map/ppermute | solution.py:296
  12.7 4.9 %collective-permute-start.3 = (s32[128]{0:T(128)S(1)}, s32[128]{0:T(128)S(1)}, u32[]{:S(2)}, u32[]{:S(2)}) collective-permute-start(s32[128]{0:T(128)S(1)} %get-tuple-element.25), channel_id=1, source_target_pairs={{4,0},{8,4},{12,8},{16,12},{20,16},{24,20},{28,24},{32,28},{36,32}... | collective-permute-start | bytes 1544 | tf_op jit(solution)/shard_map/ppermute | solution.py:299
  20.2 12.4 %copy-start.8 = (s32[96,4]{0,1:T(4,128)S(1)}, s32[96,4]{0,1:T(4,128)}, u32[]{:S(2)}) copy-start(s32[96,4]{0,1:T(4,128)} %param.25) | copy-start | bytes 4612
  20.8 78.5 %copy-start.7 = (f32[96,4]{0,1:T(4,128)S(1)}, f32[96,4]{0,1:T(4,128)}, u32[]{:S(2)}) copy-start(f32[96,4]{0,1:T(4,128)} %param.26) | copy-start | bytes 4612
  22.1 10.3 %all-to-all-start = ((bf16[4,96,256]{2,1,0:T(8,128)(2,1)}), bf16[4,96,256]{2,1,0:T(8,128)(2,1)S(1)}, u32[]{:S(2)}, u32[]{:S(2)}) async-start(bf16[4,96,256]{2,1,0:T(8,128)(2,1)} %reshape.524), calls=%async_computation | async-start | bytes 393216 | tf_op jit(solution)/shard_map/all_to_all | solution.py:405
  26.3 26.0 %collective-permute-start.4 = (bf16[2048,512]{1,0:T(8,128)(2,1)}, bf16[2048,512]{1,0:T(8,128)(2,1)S(1)}, u32[]{:S(2)}, u32[]{:S(2)}) collective-permute-start(bf16[2048,512]{1,0:T(8,128)(2,1)} %bitcast.105), channel_id=1, source_target_pairs={{0,4},{1,5},{2,1},{3,0},{4,7},{5,6},{6,2},{7,3},{8,12},{9,13},{10,... | collective-permute-start | bytes 6291464 | tf_op jit(solution)/shard_map/ppermute | solution.py:371
  32.3 42.4 %collective-permute-start.6 = (bf16[2048,512]{1,0:T(8,128)(2,1)}, bf16[2048,512]{1,0:T(8,128)(2,1)}, u32[]{:S(2)}, u32[]{:S(2)}) collective-permute-start(bf16[2048,512]{1,0:T(8,128)(2,1)} %bitcast.106), channel_id=1, source_target_pairs={{0,4},{1,5},{2,1},{3,0},{4,7},{5,6},{6,2},{7,3},{8,12},{9,13},{10,... | collective-permute-start | bytes 6291464 | tf_op jit(solution)/shard_map/ppermute | solution.py:409
  32.5 64.7 %collective-permute-start.8 = (bf16[512,2048]{1,0:T(8,128)(2,1)}, bf16[512,2048]{1,0:T(8,128)(2,1)}, u32[]{:S(2)}, u32[]{:S(2)}) collective-permute-start(bf16[512,2048]{1,0:T(8,128)(2,1)} %bitcast.107), channel_id=1, source_target_pairs={{0,4},{1,5},{2,1},{3,0},{4,7},{5,6},{6,2},{7,3},{8,12},{9,13},{10,... | collective-permute-start | bytes 6291464 | tf_op jit(solution)/shard_map/ppermute | solution.py:410
  52.2 128.7 %collective-permute-start.5 = (bf16[2048,512]{1,0:T(8,128)(2,1)S(1)}, bf16[2048,512]{1,0:T(8,128)(2,1)S(1)}, u32[]{:S(2)}, u32[]{:S(2)}) collective-permute-start(bf16[2048,512]{1,0:T(8,128)(2,1)S(1)} %collective-permute-done.4.gate_one), channel_id=1, source_target_pairs={{0,4},{1,5},{2,6},{3,7},{4,0},{5,1},{6,2},{7,3},{8,12},{9,13},{10,... | collective-permute-start | bytes 6291464 | tf_op jit(solution)/shard_map/ppermute | solution.py:411
  74.7 106.3 %collective-permute-start.7 = (bf16[2048,512]{1,0:T(8,128)(2,1)}, bf16[2048,512]{1,0:T(8,128)(2,1)S(1)}, u32[]{:S(2)}, u32[]{:S(2)}) collective-permute-start(bf16[2048,512]{1,0:T(8,128)(2,1)} %collective-permute-done.6.up_one), channel_id=1, source_target_pairs={{0,4},{1,5},{2,6},{3,7},{4,0},{5,1},{6,2},{7,3},{8,12},{9,13},{10,... | collective-permute-start | bytes 6291464 | tf_op jit(solution)/shard_map/ppermute | solution.py:423
  97.2 83.8 %collective-permute-start.9 = (bf16[512,2048]{1,0:T(8,128)(2,1)}, bf16[512,2048]{1,0:T(8,128)(2,1)S(1)}, u32[]{:S(2)}, u32[]{:S(2)}) collective-permute-start(bf16[512,2048]{1,0:T(8,128)(2,1)} %collective-permute-done.8.down_one), channel_id=1, source_target_pairs={{0,4},{1,5},{2,6},{3,7},{4,0},{5,1},{6,2},{7,3},{8,12},{9,13},{10,... | collective-permute-start | bytes 6291464 | tf_op jit(solution)/shard_map/ppermute | solution.py:424
  99.8 3.2 %copy-start.1 = (bf16[96,2048]{1,0:T(8,128)(2,1)S(1)}, bf16[96,2048]{1,0:T(8,128)(2,1)}, u32[]{:S(2)}) copy-start(bf16[96,2048]{1,0:T(8,128)(2,1)} %param.15) | copy-start | bytes 1179652
  99.8 3.2 %copy-start.3 = (f32[2048]{0:T(1024)S(1)}, f32[2048]{0:T(1024)}, u32[]{:S(2)}) copy-start(f32[2048]{0:T(1024)} %param.22) | copy-start | bytes 24580
  99.8 3.5 %copy-start.5 = (f32[2048]{0:T(1024)S(1)}, f32[2048]{0:T(1024)}, u32[]{:S(2)}) copy-start(f32[2048]{0:T(1024)} %param.23) | copy-start | bytes 24580
  179.0 1.9 copy-start
  181.0 1.4 copy-start.9
  252.3 0.7 copy-start.6
where the time goes:
time: 255 us; the launch traced here: 254 us
  Pallas kernels  144 us (56%)
  waiting for transfers between devices  63.2 us (25%)
  starting transfers between devices  25.4 us (10%)
  local copies, waits for them, and re-layouts  7.97 us (3%)
  matrix products  6.38 us (3%)
  other arithmetic  6.33 us (2%)
    pallas_call x1, Pallas kernels, dispatch(): pl.pallas_call(dispatch_kernel, out_shape=jax.ShapeDtypeStruct((4, NCOL,...  74.8 us
    pallas_call x1, Pallas kernels, expert_outputs(): pl.pallas_call(expert_kernel, out_shape=jax.ShapeDtypeStruct(half, jnp.bf...  69.5 us
    ppermute x1, waiting for transfers between devices, body(): up_one = lax.ppermute(up_weight[0], ('sp', 'tp'), first)  20.4 us
    ppermute x1, waiting for transfers between devices, body(): down_one = lax.ppermute(down_weight[0], ('sp', 'tp'), first)  20.3 us
    ppermute x1, waiting for transfers between devices, body(): gate_one = lax.ppermute(gate_weight[0], ('sp', 'tp'), first)  17.8 us
    ppermute x2, starting transfers between devices, extended(): lax.ppermute(lax.slice_in_dim(block, block.shape[dim] - width, None, axis...  8.12 us
  transfers between devices with their start and end apart: 11, of which 5 were waited for; matrix products, arithmetic and copies ran while one was open for 4% of the time, Pallas kernels for 29%

commit v1 on v0

v1 whole, which is shorter than its diff:
```python
import functools

import jax
import jax.numpy as jnp
from jax import lax
from jax.experimental import pallas as pl
from jax.experimental.pallas import tpu as pltpu
from jax.sharding import PartitionSpec as P

HD = 64
TOPK = 4
W = 128
D = 2048
CAP = 8
NZ, NX, NT = 8, 4, 4
NCOL = NZ * NX
MESH = pl.DeviceIdType.MESH

NEAR_Z = (1, 7, 2, 6, 3, 5)
OFFSETS = (
    tuple((0, dx) for dx in (1, 3, 2, 0))
    + tuple((dz, dx) for dx in (1, 3) for dz in NEAR_Z)
    + tuple((4, dx) for dx in (1, 3, 2, 0))
    + tuple((dz, dx) for dx in (2, 0) for dz in NEAR_Z)
)
SELF = OFFSETS.index((0, 0))
GROUP = 4
GROUPS = NCOL // GROUP
BACK = (4, 1, 2, 3, 5, 6, 7, 0)
TILE = 256
ROWS = 96
SPAN = 384
SLOTS = 2 * NCOL * CAP
NS = 2 * NCOL


def place():
    s = lax.axis_index("sp")
    t = lax.axis_index("tp")
    core = lax.rem(s, 2)
    column = lax.div(s, 2)
    return s, t, core, lax.div(column, NX), lax.rem(column, NX)


def shifted(z, x, core, dz, dx):
    return (lax.rem(z + dz, NZ) * NX + lax.rem(x + dx, NX)) * 2 + core


def greet(partners):
    barrier = pltpu.get_barrier_semaphore()
    for partner in partners:
        pl.semaphore_signal(barrier, inc=1, device_id=partner, device_id_type=MESH)
    pl.semaphore_wait(barrier, len(partners))


def mates(s, t):
    return [(s, lax.rem(t + step, NT)) for step in (1, 2, 3)]


def partners_of(s, t, core, z, x):
    found = mates(s, t)
    for index, (dz, dx) in enumerate(OFFSETS):
        if index != SELF:
            found.append((shifted(z, x, core, dz, dx), t))
    return found


def remote(source, target, send_sem, recv_sem, device):
    copy = pltpu.make_async_remote_copy(
        src_ref=source,
        dst_ref=target,
        send_sem=send_sem,
        recv_sem=recv_sem,
        device_id=device,
        device_id_type=MESH,
    )
    copy.start()
    return copy


def attention_kernel(
    cos_ref,
    sin_ref,
    aux_ref,
    q_hbm,
    k_hbm,
    v_hbm,
    wo_hbm,
    res_hbm,
    mix_hbm,
    ffn_hbm,
    routes_hbm,
    logits_hbm,
    gate_ref,
    up_ref,
    down_ref,
    after_ref,
    outgoing_ref,
    coarse_ref,
    fine_ref,
    gate_out,
    up_out,
    down_out,
    q_ref,
    kv_ref,
    wo_buf,
    res_ref,
    mix_ref,
    ffn_ref,
    routes_ref,
    logits_ref,
    kv_ext,
    doc_ext,
    attended,
    heads,
    normed,
    picks_buf,
    load_sem,
    halo_sem,
    head_sem,
    move_sem,
    swap_sem,
):
    s, t, core, z, x = place()
    above = (lax.rem(s + 1, NS), t)
    below = (lax.rem(s + NS - 1, NS), t)
    sibling = (s + 1 - 2 * core, t)
    keeper = core == lax.rem(t, 2)
    barrier = pltpu.get_barrier_semaphore()
    found = [above, below] + mates(s, t)
    for partner in found:
        pl.semaphore_signal(barrier, inc=1, device_id=partner, device_id_type=MESH)
    loads = [
        pltpu.make_async_copy(source, target, load_sem.at[number])
        for number, (source, target) in enumerate(
            (
                (k_hbm, kv_ref.at[pl.ds(0, HD)]),
                (v_hbm, kv_ref.at[pl.ds(HD, HD)]),
                (q_hbm, q_ref),
                (routes_hbm, routes_ref),
                (logits_hbm, logits_ref),
                (wo_hbm, wo_buf),
                (res_hbm, res_ref),
                (mix_hbm, mix_ref),
                (ffn_hbm, ffn_ref),
            )
        )
    ]
    for load in loads:
        load.start()
    pl.semaphore_wait(barrier, len(found))

    moves = {}

    def move(which):
        for side, step in ((0, 1), (1, 3)):
            neighbour = lax.rem(t + step, NT)
            half = jnp.where(keeper, side, lax.div(neighbour, 2))
            device = (jnp.where(keeper, sibling[0], s), jnp.where(keeper, t, neighbour))
            piece = pl.ds(pl.multiple_of(half * TILE, TILE), TILE)
            if which == 2:
                source, target = down_ref.at[piece, :], down_out.at[2 + side]
            elif which == 1:
                source, target = up_ref.at[:, piece], up_out.at[2 + side]
            else:
                source, target = gate_ref.at[:, piece], gate_out.at[2 + side]
            moves[which, side] = remote(
                source, target, move_sem.at[0, which, side], move_sem.at[1, which, side], device
            )

    move(0)
    move(1)
    for load in loads[:3]:
        load.wait()

    lane = lax.broadcasted_iota(jnp.int32, (128, 128), 1)
    low_half = (lane & 32) == 0
    left = lane < 64

    def turned(value, cosine, sine):
        swapped = jnp.where(low_half, pltpu.roll(value, 96, 1), pltpu.roll(value, 32, 1))
        return value * cosine + swapped * sine

    for block in (0, 2, 1):
        rows = pl.ds(block * W, W)
        pair = kv_ref[:, block * W : block * W + W].astype(jnp.float32).T
        key_turned = turned(pair, cos_ref[rows, :], sin_ref[rows, :])
        kv_ext[block + 1] = jnp.where(left, key_turned, pair).astype(jnp.bfloat16)
        doc_ext[block + 1] = aux_ref[block : block + 1, :]
    halos = [
        remote(kv_ext.at[1], kv_ext.at[4], halo_sem.at[0, 0], halo_sem.at[1, 0], below),
        remote(kv_ext.at[3], kv_ext.at[0], halo_sem.at[0, 1], halo_sem.at[1, 1], above),
        remote(doc_ext.at[1], doc_ext.at[4], halo_sem.at[0, 2], halo_sem.at[1, 2], below),
        remote(doc_ext.at[3], doc_ext.at[0], halo_sem.at[0, 3], halo_sem.at[1, 3], above),
    ]

    contract = (((1,), (1,)), ((), ()))
    for block in (1, 0, 2):
        if block == 0:
            for halo in halos:
                halo.wait_recv()
        rows = pl.ds(block * W, W)
        keys_low, keys_high, vals_low, vals_high, keep = [], [], [], [], []
        doc_query = jnp.broadcast_to(aux_ref[block : block + 1, :], (128, 128)).T
        for part in range(3):
            pair = kv_ext[block + part].astype(jnp.float32)
            other = pltpu.roll(pair, 64, 1)
            keys_low.append(jnp.where(left, pair, 0.0).astype(jnp.bfloat16))
            keys_high.append(jnp.where(left, 0.0, other).astype(jnp.bfloat16))
            vals_low.append(jnp.where(left, other, 0.0).astype(jnp.bfloat16))
            vals_high.append(jnp.where(left, 0.0, pair).astype(jnp.bfloat16))
            gap = (part - 1) * W + lane - lax.broadcasted_iota(jnp.int32, (128, 128), 0)
            place_of = s * SPAN + (block + part - 1) * W + lane
            doc_key = doc_ext[block + part]
            keep.append(
                (jnp.abs(gap) <= W)
                & (place_of >= 0)
                & (place_of < NS * SPAN)
                & (doc_query == doc_key)
            )
        keep = jnp.concatenate(keep, axis=1)
        keys_of = [jnp.concatenate(part, axis=0) for part in (keys_low, keys_high)]
        vals_of = [jnp.concatenate(part, axis=0) for part in (vals_low, vals_high)]
        for duo in range(2):
            columns = pl.ds(duo * 128, 128)
            query = turned(
                q_ref[rows, columns].astype(jnp.float32), cos_ref[rows, :], sin_ref[rows, :]
            ).astype(jnp.bfloat16)
            out = jnp.zeros((128, 128), jnp.float32)
            for side in range(2):
                head = 2 * duo + side
                scores = lax.dot_general(
                    query, keys_of[side], contract, preferred_element_type=jnp.float32
                ) * HD ** (-0.5)
                exponent = jnp.where(keep, jnp.exp(scores), 0.0)
                denominator = jnp.sum(exponent, axis=1, keepdims=True) + jnp.exp(
                    aux_ref[4 + head : 5 + head, 0:1]
                )
                probs = (exponent / denominator).astype(jnp.bfloat16)
                out = out + jnp.dot(probs, vals_of[side], preferred_element_type=jnp.float32)
            out = out.astype(jnp.bfloat16)
            for piece in range(4):
                row = block * W + piece * 32
                attended[row // ROWS, row % ROWS : row % ROWS + 32, duo * 128 : duo * 128 + 128] = (
                    out[piece * 32 : piece * 32 + 32]
                )

    swaps = []
    for step, device in zip((1, 2, 3), mates(s, t)):
        swaps.append(
            remote(
                attended.at[device[1]],
                heads.at[t],
                head_sem.at[0, step],
                head_sem.at[1, step],
                device,
            )
        )
    heads[t] = attended[t]
    move(2)
    for load in loads[3:]:
        load.wait()

    expert = routes_ref[...]
    column = lax.shift_right_logical(expert, 1)
    code = (((lax.shift_right_logical(column, 2) - z) & 7) * NX) + ((column - x) & 3)
    rank = jnp.zeros_like(code)
    for index, (dz, dx) in enumerate(OFFSETS):
        rank = jnp.where(code == dz * NX + dx, index, rank)
    rank = rank + jnp.where((expert & 1) == lax.rem(t, 2), 0, NCOL)
    weight = jnp.exp(logits_ref[...])
    weight = weight / jnp.sum(weight, axis=0, keepdims=True)
    spot = lax.broadcasted_iota(jnp.int32, (2 * NCOL, ROWS), 0)
    named = jnp.zeros((2 * NCOL, ROWS), jnp.float32)
    share = jnp.zeros((2 * NCOL, ROWS), jnp.float32)
    for choice in range(TOPK):
        hit = spot == rank[choice : choice + 1, :]
        named = jnp.where(hit, 1.0, named)
        share = jnp.where(hit, weight[choice : choice + 1, :], share)
    earlier = (
        lax.broadcasted_iota(jnp.int32, (ROWS, ROWS), 0)
        <= lax.broadcasted_iota(jnp.int32, (ROWS, ROWS), 1)
    ).astype(jnp.float32)
    counted = named * jnp.dot(
        named.astype(jnp.bfloat16),
        earlier.astype(jnp.bfloat16),
        preferred_element_type=jnp.float32,
    )
    widen = (
        lax.shift_right_logical(lax.broadcasted_iota(jnp.int32, (SLOTS, 2 * NCOL), 0), 3)
        == lax.broadcasted_iota(jnp.int32, (SLOTS, 2 * NCOL), 1)
    ).astype(jnp.float32)
    widen = widen.astype(jnp.bfloat16)
    number = (lax.broadcasted_iota(jnp.int32, (SLOTS, ROWS), 0) & 7) + 1
    picks = (
        jnp.dot(widen, counted.astype(jnp.bfloat16), preferred_element_type=jnp.float32)
        == number.astype(jnp.float32)
    )
    share_high = share.astype(jnp.bfloat16)
    share_low = (share - share_high.astype(jnp.float32)).astype(jnp.bfloat16)
    for part, target in ((share_high, coarse_ref), (share_low, fine_ref)):
        wide = jnp.dot(widen, part, preferred_element_type=jnp.float32)
        target[...] = jnp.where(picks, wide, 0.0).astype(jnp.bfloat16)
    picks_buf[...] = jnp.where(picks, 1.0, 0.0).astype(jnp.bfloat16)

    for swap in swaps:
        swap.wait_recv()

    @pl.loop(0, D // 512)
    def _(tile):
        columns = pl.ds(pl.multiple_of(tile * 512, 512), 512)
        total = jnp.zeros((ROWS, 512), jnp.float32)
        for source in range(NT):
            total = total + jnp.dot(
                heads[source],
                wo_buf[source * 256 : source * 256 + 256, columns],
                preferred_element_type=jnp.float32,
            )
        after_ref[:, columns] = total

    @pl.loop(0, ROWS // 16)
    def _(tile):
        rows = pl.ds(pl.multiple_of(tile * 16, 16), 16)
        value = rms_scale(after_ref[rows, :]) * mix_ref[...]
        value = res_ref[rows, :].astype(jnp.float32) + value
        after_ref[rows, :] = value
        normed[rows, :] = (rms_scale(value) * ffn_ref[...]).astype(jnp.bfloat16)

    @pl.loop(0, D // TILE)
    def _(tile):
        columns = pl.ds(pl.multiple_of(tile * TILE, TILE), TILE)
        outgoing_ref[:, columns] = jnp.dot(
            picks_buf[...], normed[:, columns], preferred_element_type=jnp.float32
        ).astype(jnp.bfloat16)

    trades = []
    for which, target in enumerate((gate_out, up_out, down_out)):
        for side in range(2):
            moves[which, side].wait_recv()
            trades.append(
                remote(
                    target.at[2 + side],
                    target.at[side],
                    swap_sem.at[0, which, side],
                    swap_sem.at[1, which, side],
                    sibling,
                )
            )
    for copy in trades:
        copy.wait()
    for copy in list(moves.values()) + halos + swaps:
        copy.wait_send()


def attend(*arrays):
    vmem = pl.BlockSpec(memory_space=pltpu.VMEM)
    hbm = pl.BlockSpec(memory_space=pltpu.HBM)
    dma = pltpu.SemaphoreType.DMA
    bf16 = jnp.bfloat16
    return pl.pallas_call(
        attention_kernel,
        out_shape=(
            jax.ShapeDtypeStruct((ROWS, D), jnp.float32),
            jax.ShapeDtypeStruct((SLOTS, D), bf16),
            jax.ShapeDtypeStruct((SLOTS, ROWS), bf16),
            jax.ShapeDtypeStruct((SLOTS, ROWS), bf16),
            jax.ShapeDtypeStruct((4, D, TILE), bf16),
            jax.ShapeDtypeStruct((4, D, TILE), bf16),
            jax.ShapeDtypeStruct((4, TILE, D), bf16),
        ),
        in_specs=[vmem] * 3 + [hbm] * 12,
        out_specs=(vmem,) * 4 + (hbm,) * 3,
        scratch_shapes=[
            pltpu.VMEM((SPAN, 256), bf16),
            pltpu.VMEM((2 * HD, SPAN), bf16),
            pltpu.VMEM((1024, D), bf16),
            pltpu.VMEM((ROWS, D), bf16),
            pltpu.VMEM((1, D), jnp.float32),
            pltpu.VMEM((1, D), jnp.float32),
            pltpu.VMEM((TOPK, ROWS), jnp.int32),
            pltpu.VMEM((TOPK, ROWS), jnp.float32),
            pltpu.VMEM((5, W, 128), bf16),
            pltpu.VMEM((5, 1, 128), jnp.float32),
            pltpu.VMEM((NT, ROWS, 256), bf16),
            pltpu.VMEM((NT, ROWS, 256), bf16),
            pltpu.VMEM((ROWS, D), bf16),
            pltpu.VMEM((SLOTS, ROWS), bf16),
            dma((9,)),
            dma((2, 4)),
            dma((2, 4)),
            dma((2, 3, 2)),
            dma((2, 3, 2)),
        ],
        compiler_params=pltpu.CompilerParams(
            collective_id=2, has_side_effects=True, vmem_limit_bytes=60 << 20
        ),
        cost_estimate=pl.CostEstimate(
            flops=1_000_000_000, bytes_accessed=100_000_000, transcendentals=0
        ),
    )(*arrays)


def dispatch_kernel(out_ref, in_ref, transit, send_sem, recv_sem, own_sem, far_sem):
    s, t, core, z, x = place()
    near, far, back = mates(s, t)
    greet(partners_of(s, t, core, z, x))
    arrived = {}
    for index, (dz, dx) in enumerate(OFFSETS):
        for kind in range(2):
            target = in_ref.at[0, index] if kind == 0 else transit.at[index]
            if index == SELF:
                copy = pltpu.make_async_copy(out_ref.at[kind, index], target, own_sem.at[kind])
                copy.start()
            else:
                copy = remote(
                    out_ref.at[kind, index],
                    target,
                    send_sem.at[kind, index],
                    recv_sem.at[kind, index],
                    (shifted(z, x, core, dz, dx), t),
                )
            arrived[kind, index] = copy
    forwards = []
    for group in range(GROUPS):
        block = pl.ds(group * GROUP, GROUP)
        for kind in range(2):
            for index in range(group * GROUP, (group + 1) * GROUP):
                if index == SELF:
                    arrived[kind, index].wait()
                else:
                    arrived[kind, index].wait_recv()
            if kind == 0:
                routes = ((in_ref.at[0, block], 1, far),)
            else:
                routes = ((transit.at[block], 3, near), (transit.at[block], 2, back))
            for source, slot, device in routes:
                forwards.append(
                    remote(
                        source,
                        in_ref.at[slot, block],
                        far_sem.at[0, slot, group],
                        far_sem.at[1, slot, group],
                        device,
                    )
                )
    for (kind, index), copy in arrived.items():
        if index != SELF:
            copy.wait_send()
    for copy in forwards:
        copy.wait()


def dispatch(outgoing):
    return pl.pallas_call(
        dispatch_kernel,
        out_shape=jax.ShapeDtypeStruct((4, NCOL, CAP, D), jnp.bfloat16),
        in_specs=[pl.BlockSpec(memory_space=pltpu.VMEM)],
        out_specs=pl.BlockSpec(memory_space=pl.ANY),
        scratch_shapes=[
            pltpu.VMEM((NCOL, CAP, D), jnp.bfloat16),
            pltpu.SemaphoreType.DMA((2, NCOL)),
            pltpu.SemaphoreType.DMA((2, NCOL)),
            pltpu.SemaphoreType.DMA((2,)),
            pltpu.SemaphoreType.DMA((2, 4, GROUPS)),
        ],
        compiler_params=pltpu.CompilerParams(
            collective_id=0, has_side_effects=True, vmem_limit_bytes=58 << 20
        ),
        cost_estimate=pl.CostEstimate(flops=0, bytes_accessed=150_000_000, transcendentals=0),
    )(outgoing)


def expert_kernel(
    rows_ref,
    gate_hbm,
    up_hbm,
    down_hbm,
    ret_ref,
    gate_ref,
    up_ref,
    down_ref,
    block_rows,
    hidden,
    mine,
    away,
    theirs,
    total,
    load_sem,
    pair_sem,
    send_sem,
    recv_sem,
):
    s, t, core, z, x = place()
    near, far, back = mates(s, t)
    loads = [
        pltpu.make_async_copy(source, target, load_sem.at[number])
        for number, (source, target) in enumerate(
            ((gate_hbm, gate_ref), (up_hbm, up_ref), (down_hbm, down_ref))
        )
    ]
    for load in loads:
        load.start()
    greet(partners_of(s, t, core, z, x))
    for load in loads:
        load.wait()
    count = 4 * GROUP * CAP
    pairs = {}
    sends = []
    own = []

    def compute(group):
        block = pl.ds(group * GROUP, GROUP)
        block_rows[...] = (
            rows_ref[:, block].astype(jnp.float32).reshape(count, D).astype(jnp.bfloat16)
        )

        @pl.loop(0, 4)
        def _(part):
            gate_pre = jnp.dot(block_rows[...], gate_ref[part], preferred_element_type=jnp.float32)
            up_pre = jnp.dot(block_rows[...], up_ref[part], preferred_element_type=jnp.float32)
            gated = jnp.minimum(gate_pre, 7.0)
            upper = jnp.clip(up_pre, -7.0, 7.0)
            value = (upper + 1.0) * gated * jax.nn.sigmoid(1.702 * gated)
            hidden[part] = value.astype(jnp.bfloat16)

        @pl.loop(0, D // TILE)
        def _(column):
            columns = pl.ds(pl.multiple_of(column * TILE, TILE), TILE)
            term = jnp.zeros((count, TILE), jnp.float32)
            for part in range(4):
                term = term + jnp.dot(
                    hidden[part], down_ref[part, :, columns], preferred_element_type=jnp.float32
                )
            term = term.reshape(4, GROUP, CAP, TILE).astype(jnp.bfloat16)
            mine[block, :, columns] = term[0]
            away[:, block, :, columns] = term[1:]

    def swap(group):
        block = pl.ds(group * GROUP, GROUP)
        for source, slot, device in ((1, 1, near), (2, 2, back), (0, 0, far)):
            pairs[slot, group] = remote(
                away.at[source, block],
                theirs.at[slot, block],
                pair_sem.at[0, slot, group],
                pair_sem.at[1, slot, group],
                device,
            )

    def add(group):
        block = pl.ds(group * GROUP, GROUP)
        for slot in range(3):
            pairs[slot, group].wait_recv()
        total[1, block] = (
            theirs[1, block].astype(jnp.float32) + theirs[2, block].astype(jnp.float32)
        ).astype(jnp.bfloat16)
        total[0, block] = (
            mine[block].astype(jnp.float32) + theirs[0, block].astype(jnp.float32)
        ).astype(jnp.bfloat16)

    def home(group):
        for kind in (1, 0):
            for index in range(group * GROUP, (group + 1) * GROUP):
                dz, dx = OFFSETS[index]
                if index == SELF:
                    copy = pltpu.make_async_copy(
                        total.at[kind, index], ret_ref.at[kind, index], send_sem.at[kind, index]
                    )
                    copy.start()
                    own.append(copy)
                else:
                    sends.append(
                        remote(
                            total.at[kind, index],
                            ret_ref.at[kind, index],
                            send_sem.at[kind, index],
                            recv_sem.at[kind, index],
                            (shifted(z, x, core, NZ - dz, NX - dx), t),
                        )
                    )

    behind = 2
    for step in range(GROUPS + behind):
        if step < GROUPS:
            compute(BACK[step])
        if step >= behind:
            add(BACK[step - behind])
        if step < GROUPS:
            swap(BACK[step])
        if step >= behind:
            home(BACK[step - behind])
    for copy in pairs.values():
        copy.wait_send()
    for copy in own:
        copy.wait()
    for copy in sends:
        copy.wait()


def expert_outputs(rows_in, gate, up, down):
    half = (2, NCOL, CAP, D)
    third = (3, NCOL, CAP, D)
    count = 4 * GROUP * CAP
    vmem = pl.BlockSpec(memory_space=pltpu.VMEM)
    return pl.pallas_call(
        expert_kernel,
        out_shape=jax.ShapeDtypeStruct(half, jnp.bfloat16),
        in_specs=[vmem] + [pl.BlockSpec(memory_space=pltpu.HBM)] * 3,
        out_specs=pl.BlockSpec(memory_space=pl.ANY),
        scratch_shapes=[
            pltpu.VMEM((4, D, TILE), jnp.bfloat16),
            pltpu.VMEM((4, D, TILE), jnp.bfloat16),
            pltpu.VMEM((4, TILE, D), jnp.bfloat16),
            pltpu.VMEM((count, D), jnp.bfloat16),
            pltpu.VMEM((4, count, TILE), jnp.bfloat16),
            pltpu.VMEM((NCOL, CAP, D), jnp.bfloat16),
            pltpu.VMEM(third, jnp.bfloat16),
            pltpu.VMEM(third, jnp.bfloat16),
            pltpu.VMEM(half, jnp.bfloat16),
            pltpu.SemaphoreType.DMA((3,)),
            pltpu.SemaphoreType.DMA((2, 3, GROUPS)),
            pltpu.SemaphoreType.DMA((2, NCOL)),
            pltpu.SemaphoreType.DMA((2, NCOL)),
        ],
        compiler_params=pltpu.CompilerParams(
            collective_id=1, has_side_effects=True, vmem_limit_bytes=58 << 20
        ),
        cost_estimate=pl.CostEstimate(
            flops=13_000_000_000, bytes_accessed=150_000_000, transcendentals=0
        ),
    )(rows_in, gate, up, down)


def rms_scale(vector):
    return vector * lax.rsqrt(jnp.mean(vector * vector, axis=-1, keepdims=True) + 1e-06)


def body(
    residual,
    queries,
    keys,
    values,
    documents,
    sink,
    out_weight,
    mix_gain,
    ffn_gain,
    out_gain,
    routes,
    route_logits,
    gate_weight,
    up_weight,
    down_weight,
):
    positions = lax.axis_index("sp") * SPAN + jnp.arange(SPAN, dtype=jnp.int32)
    half_size = HD // 2
    lanes = jnp.arange(128, dtype=jnp.int32)
    inverse = 10000.0 ** (-(lanes % half_size).astype(jnp.float32) / half_size)
    angles = positions.astype(jnp.float32)[:, None] * inverse[None, :]
    sign = jnp.where(lanes % HD < half_size, -1.0, 1.0)
    cosine, sine = jnp.cos(angles), jnp.sin(angles) * sign[None, :]
    aux = jnp.concatenate(
        [
            documents.astype(jnp.float32).reshape(SPAN // W, W),
            jnp.zeros((1, W), jnp.float32),
            jnp.broadcast_to(sink[:, None], (4, W)),
        ],
        axis=0,
    )
    after_mix, outgoing, coarse, fine, gate, up, down = attend(
        cosine,
        sine,
        aux,
        queries,
        keys.T,
        values.T,
        out_weight,
        residual,
        mix_gain.reshape(1, D),
        ffn_gain.reshape(1, D),
        routes.T,
        route_logits.T,
        gate_weight[0],
        up_weight[0],
        down_weight[0],
    )
    rows_in = dispatch(outgoing.reshape(2, NCOL, CAP, D))
    returned = expert_outputs(rows_in, gate, up, down).reshape(SLOTS, D)
    contract = (((0,), (0,)), ((), ()))
    expert_mix = lax.dot_general(
        coarse, returned, contract, preferred_element_type=jnp.float32
    ) + lax.dot_general(fine, returned, contract, preferred_element_type=jnp.float32)
    return (after_mix + rms_scale(expert_mix) * out_gain).astype(jnp.bfloat16)


def solution(mesh):
    in_specs = (
        P(("sp", "tp"), None),
        P("sp", "tp"),
        P("sp", "tp"),
        P("sp", "tp"),
        P("sp"),
        P("tp"),
        P(),
        P(),
        P(),
        P(),
        P(("sp", "tp"), None),
        P(("sp", "tp"), None),
        P("sp", None, "tp"),
        P("sp", None, "tp"),
        P("sp", "tp", None),
    )
    out_specs = P(("sp", "tp"), None)
    return jax.shard_map(body, mesh=mesh, in_specs=in_specs, out_specs=out_specs, check_vma=False)
```

time: 255 us -> 201 us (0.79)
  waiting for transfers between devices: 63.2 us -> 0 us
  Pallas kernels: 144 us -> 192 us
  starting transfers between devices: 25.4 us -> 0 us
  local copies, waits for them, and re-layouts: 7.97 us -> 1.33 us
  matrix products: 6.38 us -> 2.83 us
    ppermute x10 -> x0, waiting for transfers between devices: 59.8 us -> none  [the longest x1 20.4 us: body(): up_one = lax.ppermute(up_weight[0], ('sp', 'tp'), first)]
    pallas_call x0 -> x1, Pallas kernels: none -> 56.8 us  [attend(): pl.pallas_call(attention_kernel, out_shape=(jax.ShapeDtypeStruct((ROWS, D...]
    ppermute x10 -> x0, starting transfers between devices: 21.2 us -> none  [the longest x2 8.12 us: extended(): lax.ppermute(lax.slice_in_dim(block, block.shape[dim] - width, None, axis...]
    pallas_call x1, Pallas kernels: 74.8 us -> 66.2 us  [dispatch(): pl.pallas_call(dispatch_kernel, out_shape=jax.ShapeDtypeStruct((4, NCOL,...]
    all_to_all x1 -> x0, starting transfers between devices: 4.18 us -> none  [body(): lax.all_to_all(attended, 'tp', split_axis=0, concat_axis=1, tiled=True)]
    unnamed x24 -> x10, local copies, waits for them, and re-layouts: 4.61 us -> 0.53 us
    dot_general x6 -> x2, matrix products: 6.38 us -> 2.83 us  [the longest x1 2.24 us: body(): lax.dot_general(coarse, returned, contract, preferred_element_type=jnp.fl...]
    all_to_all x1 -> x0, waiting for transfers between devices: 3.39 us -> none  [body(): lax.all_to_all(attended, 'tp', split_axis=0, concat_axis=1, tiled=True)]
  transfers between devices with their start and end apart: 11 -> 0, of which waited for: 5 -> 0; matrix products, arithmetic and copies ran while one was open for 4% -> 0% of each run, Pallas kernels for 29% -> 0%
where the time goes in v1:
time: 201 us; the launch traced here: 200 us
  Pallas kernels  192 us (96%)
  other arithmetic  3.79 us (2%)
  matrix products  2.83 us (1%)
    pallas_call x1, Pallas kernels, expert_outputs(): pl.pallas_call(expert_kernel, out_shape=jax.ShapeDtypeStruct(half, jnp.bf...  69.3 us
    pallas_call x1, Pallas kernels, dispatch(): pl.pallas_call(dispatch_kernel, out_shape=jax.ShapeDtypeStruct((4, NCOL,...  66.2 us
    pallas_call x1, Pallas kernels, attend(): pl.pallas_call(attention_kernel, out_shape=(jax.ShapeDtypeStruct((ROWS, D...  56.8 us

profile of v1, /device:TPU:1, one launch (start us, length us, event | category | flops | bytes accessed | tf_op | source)
XLA Modules:
  0.0 200.3 jit_solution(3311910347335025083)
XLA Ops:
  0.0 0.7 pad.2.clone
  0.7 0.1 pad.1.clone
  0.8 0.7 convert_bitcast_fusion
  1.5 0.7 maximum_maximum_fusion.aux_ref
  2.2 1.5 fusion
  3.7 56.8 %shard_map.145 = (f32[96,2048]{1,0:T(8,128)}, bf16[512,2048]{1,0:T(8,128)(2,1)}, bf16[512,96]{1,0:T(8,128)(2,1)}, bf16[512,96]{1,0:T(8,128)(2,1)}, bf16[4,2048,2...) custom-call(f32[384,128]{1,0:T(8,128)} %get-tuple-element.20.cos_ref, ...), custom_call_target="tpu_custom_call" | custom-call | flops 1000000000 | bytes 100000000 | tf_op jit(solution)/shard_map/pallas_call | solution.py:360
  60.5 66.2 %shard_map.146.rows_ref = bf16[4,32,8,2048]{3,2,1,0:T(8,128)(2,1)} custom-call(bf16[2,32,8,2048]{3,2,1,0:T(8,128)(2,1)} %bitcast.23), custom_call_target="tpu_custom_call" | custom-call | bytes 150000000 | tf_op jit(solution)/shard_map/pallas_call | solution.py:454
  126.7 0.0 copy-start.3
  126.7 69.3 %shard_map.147 = bf16[2,32,8,2048]{3,2,1,0:T(8,128)(2,1)} custom-call(bf16[4,32,8,2048]{3,2,1,0:T(8,128)(2,1)} %shard_map.146.rows_ref, bf16[4,2048,256]{2,1,0:T(8,128)(2,1)} %get-tuple-element.15.gate_hbm, bf16[4,2048,256]{2,1,0:T(8,128)(2,1)} %get-tuple-element.16.up_hbm, bf16[4,256,2048]{2,1,0:T(8,128)(2,1)} %get-tuple-element.17.down_hbm), custom_call_target="tpu_custom_call" | custom-call | flops 12999999488 | bytes 150000000 | tf_op jit(solution)/shard_map/pallas_call | solution.py:604
  196.0 0.0 copy-start
  196.0 0.0 copy-start.2
  196.0 0.0 copy-done.3
  196.0 2.2 %fusion.5 = f32[96,2048]{1,0:T(8,128)S(1)} fusion(bf16[512,96]{1,0:T(8,128)(2,1)S(1)} %copy-done.3, bf16[512,2048]{1,0:T(8,128)(2,1)} %bitcast.18), kind=kOutput, calls=%fused_computation.17 | convolution fusion | flops 201326592 | bytes 2981888 | tf_op jit(solution)/shard_map/dot_general | solution.py:689
  198.3 0.0 copy-done
  198.3 0.0 copy-done.2
  198.3 0.0 copy-start.1
  198.3 0.0 copy-start.4
  198.3 0.6 multiply_reduce_fusion
  198.9 0.5 copy-done.1
  199.4 0.0 copy-done.4
  199.4 0.9 add_convert_fusion
  (3 shorter events, 0.0 us)
Async XLA Ops:
  126.7 69.3 %copy-start.3 = (bf16[512,96]{1,0:T(8,128)(2,1)S(1)}, bf16[512,96]{1,0:T(8,128)(2,1)}, u32[]{:S(2)}) copy-start(bf16[512,96]{1,0:T(8,128)(2,1)} %get-tuple-element.13) | copy-start | bytes 294916
  196.0 2.3 %copy-start = (bf16[2,32,8,2048]{3,2,1,0:T(8,128)(2,1)S(1)}, bf16[2,32,8,2048]{3,2,1,0:T(8,128)(2,1)}, u32[]{:S(2)}) copy-start(bf16[2,32,8,2048]{3,2,1,0:T(8,128)(2,1)} %shard_map.147) | copy-start | bytes 6291460
  196.0 2.3 %copy-start.2 = (bf16[512,96]{1,0:T(8,128)(2,1)S(1)}, bf16[512,96]{1,0:T(8,128)(2,1)}, u32[]{:S(2)}) copy-start(bf16[512,96]{1,0:T(8,128)(2,1)} %get-tuple-element.18) | copy-start | bytes 294916
  198.3 1.1 copy-start.1
  198.3 1.1 copy-start.4

commit v2 on v1

--- a/solution.py
+++ b/solution.py
@@ -1,5 +1,3 @@
-import functools
-
 import jax
 import jax.numpy as jnp
 from jax import lax
@@ -18,15 +16,14 @@
 
 NEAR_Z = (1, 7, 2, 6, 3, 5)
 OFFSETS = (
-    tuple((0, dx) for dx in (1, 3, 2, 0))
+    ((0, 1), (0, 3))
     + tuple((dz, dx) for dx in (1, 3) for dz in NEAR_Z)
     + tuple((4, dx) for dx in (1, 3, 2, 0))
     + tuple((dz, dx) for dx in (2, 0) for dz in NEAR_Z)
+    + ((0, 2), (0, 0))
 )
 SELF = OFFSETS.index((0, 0))
-GROUP = 4
-GROUPS = NCOL // GROUP
-BACK = (4, 1, 2, 3, 5, 6, 7, 0)
+SPLIT = ((0, 2),) + tuple((start, 4) for start in range(2, 30, 4)) + ((30, 2),)
 TILE = 256
 ROWS = 96
 SPAN = 384
@@ -44,13 +41,6 @@
 
 def shifted(z, x, core, dz, dx):
     return (lax.rem(z + dz, NZ) * NX + lax.rem(x + dx, NX)) * 2 + core
-
-
-def greet(partners):
-    barrier = pltpu.get_barrier_semaphore()
-    for partner in partners:
-        pl.semaphore_signal(barrier, inc=1, device_id=partner, device_id_type=MESH)
-    pl.semaphore_wait(barrier, len(partners))
 
 
 def mates(s, t):
@@ -78,7 +68,7 @@
     return copy
 
 
-def attention_kernel(
+def layer_kernel(
     cos_ref,
     sin_ref,
     aux_ref,
@@ -91,16 +81,13 @@
     ffn_hbm,
     routes_hbm,
     logits_hbm,
-    gate_ref,
-    up_ref,
-    down_ref,
+    gate_hbm,
+    up_hbm,
+    down_hbm,
     after_ref,
-    outgoing_ref,
     coarse_ref,
     fine_ref,
-    gate_out,
-    up_out,
-    down_out,
+    ret_ref,
     q_ref,
     kv_ref,
     wo_buf,
@@ -115,11 +102,30 @@
     heads,
     normed,
     picks_buf,
+    out_ref,
+    gate_ref,
+    up_ref,
+    down_ref,
+    rows_ref,
+    transit,
+    block_rows,
+    hidden,
+    mine,
+    away,
+    theirs,
+    total,
     load_sem,
     halo_sem,
     head_sem,
     move_sem,
     swap_sem,
+    go_send_sem,
+    go_recv_sem,
+    own_sem,
+    far_sem,
+    pair_sem,
+    send_sem,
+    recv_sem,
 ):
     s, t, core, z, x = place()
     above = (lax.rem(s + 1, NS), t)
@@ -127,7 +133,8 @@
     sibling = (s + 1 - 2 * core, t)
     keeper = core == lax.rem(t, 2)
     barrier = pltpu.get_barrier_semaphore()
-    found = [above, below] + mates(s, t)
+    near, far, back = mates(s, t)
+    found = [above, below] + partners_of(s, t, core, z, x)
     for partner in found:
         pl.semaphore_signal(barrier, inc=1, device_id=partner, device_id_type=MESH)
     loads = [
@@ -159,11 +166,11 @@
             device = (jnp.where(keeper, sibling[0], s), jnp.where(keeper, t, neighbour))
             piece = pl.ds(pl.multiple_of(half * TILE, TILE), TILE)
             if which == 2:
-                source, target = down_ref.at[piece, :], down_out.at[2 + side]
+                source, target = down_hbm.at[piece, :], down_ref.at[2 + side]
             elif which == 1:
-                source, target = up_ref.at[:, piece], up_out.at[2 + side]
+                source, target = up_hbm.at[:, piece], up_ref.at[2 + side]
             else:
-                source, target = gate_ref.at[:, piece], gate_out.at[2 + side]
+                source, target = gate_hbm.at[:, piece], gate_ref.at[2 + side]
             moves[which, side] = remote(
                 source, target, move_sem.at[0, which, side], move_sem.at[1, which, side], device
             )
@@ -329,12 +336,13 @@
     @pl.loop(0, D // TILE)
     def _(tile):
         columns = pl.ds(pl.multiple_of(tile * TILE, TILE), TILE)
-        outgoing_ref[:, columns] = jnp.dot(
-            picks_buf[...], normed[:, columns], preferred_element_type=jnp.float32
-        ).astype(jnp.bfloat16)
+        packed = jnp.dot(picks_buf[...], normed[:, columns], preferred_element_type=jnp.float32)
+        out_ref[:, :, :, columns] = packed.reshape(2, NCOL, CAP, TILE).astype(jnp.bfloat16)
 
     trades = []
-    for which, target in enumerate((gate_out, up_out, down_out)):
+
+    def trade(which):
+        target = (gate_ref, up_ref, down_ref)[which]
         for side in range(2):
             moves[which, side].wait_recv()
             trades.append(
@@ -346,68 +354,14 @@
                     sibling,
                 )
             )
-    for copy in trades:
-        copy.wait()
-    for copy in list(moves.values()) + halos + swaps:
-        copy.wait_send()
-
-
-def attend(*arrays):
-    vmem = pl.BlockSpec(memory_space=pltpu.VMEM)
-    hbm = pl.BlockSpec(memory_space=pltpu.HBM)
-    dma = pltpu.SemaphoreType.DMA
-    bf16 = jnp.bfloat16
-    return pl.pallas_call(
-        attention_kernel,
-        out_shape=(
-            jax.ShapeDtypeStruct((ROWS, D), jnp.float32),
-            jax.ShapeDtypeStruct((SLOTS, D), bf16),
-            jax.ShapeDtypeStruct((SLOTS, ROWS), bf16),
-            jax.ShapeDtypeStruct((SLOTS, ROWS), bf16),
-            jax.ShapeDtypeStruct((4, D, TILE), bf16),
-            jax.ShapeDtypeStruct((4, D, TILE), bf16),
-            jax.ShapeDtypeStruct((4, TILE, D), bf16),
-        ),
-        in_specs=[vmem] * 3 + [hbm] * 12,
-        out_specs=(vmem,) * 4 + (hbm,) * 3,
-        scratch_shapes=[
-            pltpu.VMEM((SPAN, 256), bf16),
-            pltpu.VMEM((2 * HD, SPAN), bf16),
-            pltpu.VMEM((1024, D), bf16),
-            pltpu.VMEM((ROWS, D), bf16),
-            pltpu.VMEM((1, D), jnp.float32),
-            pltpu.VMEM((1, D), jnp.float32),
-            pltpu.VMEM((TOPK, ROWS), jnp.int32),
-            pltpu.VMEM((TOPK, ROWS), jnp.float32),
-            pltpu.VMEM((5, W, 128), bf16),
-            pltpu.VMEM((5, 1, 128), jnp.float32),
-            pltpu.VMEM((NT, ROWS, 256), bf16),
-            pltpu.VMEM((NT, ROWS, 256), bf16),
-            pltpu.VMEM((ROWS, D), bf16),
-            pltpu.VMEM((SLOTS, ROWS), bf16),
-            dma((9,)),
-            dma((2, 4)),
-            dma((2, 4)),
-            dma((2, 3, 2)),
-            dma((2, 3, 2)),
-        ],
-        compiler_params=pltpu.CompilerParams(
-            collective_id=2, has_side_effects=True, vmem_limit_bytes=60 << 20
-        ),
-        cost_estimate=pl.CostEstimate(
-            flops=1_000_000_000, bytes_accessed=100_000_000, transcendentals=0
-        ),
-    )(*arrays)
-
-
-def dispatch_kernel(out_ref, in_ref, transit, send_sem, recv_sem, own_sem, far_sem):
-    s, t, core, z, x = place()
-    near, far, back = mates(s, t)
-    greet(partners_of(s, t, core, z, x))
-    arrived = {}
+
+    trade(0)
+    trade(1)
+
+    arrived, forwards, pairs, sends, own = {}, {}, {}, [], []
     for index, (dz, dx) in enumerate(OFFSETS):
         for kind in range(2):
-            target = in_ref.at[0, index] if kind == 0 else transit.at[index]
+            target = rows_ref.at[0, index] if kind == 0 else transit.at[index]
             if index == SELF:
                 copy = pltpu.make_async_copy(out_ref.at[kind, index], target, own_sem.at[kind])
                 copy.start()
@@ -415,113 +369,54 @@
                 copy = remote(
                     out_ref.at[kind, index],
                     target,
-                    send_sem.at[kind, index],
-                    recv_sem.at[kind, index],
+                    go_send_sem.at[kind, index],
+                    go_recv_sem.at[kind, index],
                     (shifted(z, x, core, dz, dx), t),
                 )
             arrived[kind, index] = copy
-    forwards = []
-    for group in range(GROUPS):
-        block = pl.ds(group * GROUP, GROUP)
+
+    def forward(group):
+        start, size = SPLIT[group]
+        block = pl.ds(start, size)
         for kind in range(2):
-            for index in range(group * GROUP, (group + 1) * GROUP):
+            for index in range(start, start + size):
                 if index == SELF:
                     arrived[kind, index].wait()
                 else:
                     arrived[kind, index].wait_recv()
             if kind == 0:
-                routes = ((in_ref.at[0, block], 1, far),)
+                routes = ((rows_ref.at[0, block], 1, far),)
             else:
                 routes = ((transit.at[block], 3, near), (transit.at[block], 2, back))
             for source, slot, device in routes:
-                forwards.append(
-                    remote(
-                        source,
-                        in_ref.at[slot, block],
-                        far_sem.at[0, slot, group],
-                        far_sem.at[1, slot, group],
-                        device,
-                    )
+                forwards[slot, group] = remote(
+                    source,
+                    rows_ref.at[slot, block],
+                    far_sem.at[0, slot - 1, group],
+                    far_sem.at[1, slot - 1, group],
+                    device,
                 )
-    for (kind, index), copy in arrived.items():
-        if index != SELF:
-            copy.wait_send()
-    for copy in forwards:
-        copy.wait()
-
-
-def dispatch(outgoing):
-    return pl.pallas_call(
-        dispatch_kernel,
-        out_shape=jax.ShapeDtypeStruct((4, NCOL, CAP, D), jnp.bfloat16),
-        in_specs=[pl.BlockSpec(memory_space=pltpu.VMEM)],
-        out_specs=pl.BlockSpec(memory_space=pl.ANY),
-        scratch_shapes=[
-            pltpu.VMEM((NCOL, CAP, D), jnp.bfloat16),
-            pltpu.SemaphoreType.DMA((2, NCOL)),
-            pltpu.SemaphoreType.DMA((2, NCOL)),
-            pltpu.SemaphoreType.DMA((2,)),
-            pltpu.SemaphoreType.DMA((2, 4, GROUPS)),
-        ],
-        compiler_params=pltpu.CompilerParams(
-            collective_id=0, has_side_effects=True, vmem_limit_bytes=58 << 20
-        ),
-        cost_estimate=pl.CostEstimate(flops=0, bytes_accessed=150_000_000, transcendentals=0),
-    )(outgoing)
-
-
-def expert_kernel(
-    rows_ref,
-    gate_hbm,
-    up_hbm,
-    down_hbm,
-    ret_ref,
-    gate_ref,
-    up_ref,
-    down_ref,
-    block_rows,
-    hidden,
-    mine,
-    away,
-    theirs,
-    total,
-    load_sem,
-    pair_sem,
-    send_sem,
-    recv_sem,
-):
-    s, t, core, z, x = place()
-    near, far, back = mates(s, t)
-    loads = [
-        pltpu.make_async_copy(source, target, load_sem.at[number])
-        for number, (source, target) in enumerate(
-            ((gate_hbm, gate_ref), (up_hbm, up_ref), (down_hbm, down_ref))
-        )
-    ]
-    for load in loads:
-        load.start()
-    greet(partners_of(s, t, core, z, x))
-    for load in loads:
-        load.wait()
-    count = 4 * GROUP * CAP
-    pairs = {}
-    sends = []
-    own = []
 
     def compute(group):
-        block = pl.ds(group * GROUP, GROUP)
-        block_rows[...] = (
+        start, size = SPLIT[group]
+        block = pl.ds(start, size)
+        count = 4 * size * CAP
+        for slot in (1, 2, 3):
+            forwards[slot, group].wait_recv()
+        block_rows[:count] = (
             rows_ref[:, block].astype(jnp.float32).reshape(count, D).astype(jnp.bfloat16)
         )
 
         @pl.loop(0, 4)
         def _(part):
-            gate_pre = jnp.dot(block_rows[...], gate_ref[part], preferred_element_type=jnp.float32)
-            up_pre = jnp.dot(block_rows[...], up_ref[part], preferred_element_type=jnp.float32)
+            gate_pre = jnp.dot(
+                block_rows[:count], gate_ref[part], preferred_element_type=jnp.float32
+            )
+            up_pre = jnp.dot(block_rows[:count], up_ref[part], preferred_element_type=jnp.float32)
             gated = jnp.minimum(gate_pre, 7.0)
             upper = jnp.clip(up_pre, -7.0, 7.0)
             value = (upper + 1.0) * gated * jax.nn.sigmoid(1.702 * gated)
-            hidden[part] = value.astype(jnp.bfloat16)
+            hidden[part, :count] = value.astype(jnp.bfloat16)
 
         @pl.loop(0, D // TILE)
         def _(column):
@@ -529,14 +424,17 @@
             term = jnp.zeros((count, TILE), jnp.float32)
             for part in range(4):
                 term = term + jnp.dot(
-                    hidden[part], down_ref[part, :, columns], preferred_element_type=jnp.float32
+                    hidden[part, :count],
+                    down_ref[part, :, columns],
+                    preferred_element_type=jnp.float32,
                 )
-            term = term.reshape(4, GROUP, CAP, TILE).astype(jnp.bfloat16)
+            term = term.reshape(4, size, CAP, TILE).astype(jnp.bfloat16)
             mine[block, :, columns] = term[0]
             away[:, block, :, columns] = term[1:]
 
     def swap(group):
-        block = pl.ds(group * GROUP, GROUP)
+        start, size = SPLIT[group]
+        block = pl.ds(start, size)
         for source, slot, device in ((1, 1, near), (2, 2, back), (0, 0, far)):
             pairs[slot, group] = remote(
                 away.at[source, block],
@@ -547,7 +445,8 @@
             )
 
     def add(group):
-        block = pl.ds(group * GROUP, GROUP)
+        start, size = SPLIT[group]
+        block = pl.ds(start, size)
         for slot in range(3):
             pairs[slot, group].wait_recv()
         total[1, block] = (
@@ -558,8 +457,9 @@
         ).astype(jnp.bfloat16)
 
     def home(group):
+        start, size = SPLIT[group]
         for kind in (1, 0):
-            for index in range(group * GROUP, (group + 1) * GROUP):
+            for index in range(start, start + size):
                 dz, dx = OFFSETS[index]
                 if index == SELF:
                     copy = pltpu.make_async_copy(
@@ -578,17 +478,29 @@
                         )
                     )
 
-    behind = 2
-    for step in range(GROUPS + behind):
-        if step < GROUPS:
-            compute(BACK[step])
-        if step >= behind:
-            add(BACK[step - behind])
-        if step < GROUPS:
-            swap(BACK[step])
-        if step >= behind:
-            home(BACK[step - behind])
-    for copy in pairs.values():
+    last = len(SPLIT)
+    for step in range(last + 3):
+        if step < last:
+            forward(step)
+        if step == 0:
+            trade(2)
+        if step == 1:
+            for copy in trades:
+                copy.wait_recv()
+        if 1 <= step <= last:
+            compute(step - 1)
+        if step >= 3:
+            add(step - 3)
+        if 1 <= step <= last:
+            swap(step - 1)
+        if step >= 3:
+            home(step - 3)
+    for (kind, index), copy in arrived.items():
+        if index != SELF:
+            copy.wait_send()
+    for copy in list(forwards.values()) + list(pairs.values()) + trades:
+        copy.wait_send()
+    for copy in list(moves.values()) + halos + swaps:
         copy.wait_send()
     for copy in own:
         copy.wait()
@@ -596,38 +508,71 @@
         copy.wait()
 
 
-def expert_outputs(rows_in, gate, up, down):
+def layer(*arrays):
+    vmem = pl.BlockSpec(memory_space=pltpu.VMEM)
+    hbm = pl.BlockSpec(memory_space=pltpu.HBM)
+    dma = pltpu.SemaphoreType.DMA
+    bf16 = jnp.bfloat16
     half = (2, NCOL, CAP, D)
     third = (3, NCOL, CAP, D)
-    count = 4 * GROUP * CAP
-    vmem = pl.BlockSpec(memory_space=pltpu.VMEM)
+    count = 4 * max(size for _, size in SPLIT) * CAP
     return pl.pallas_call(
-        expert_kernel,
-        out_shape=jax.ShapeDtypeStruct(half, jnp.bfloat16),
-        in_specs=[vmem] + [pl.BlockSpec(memory_space=pltpu.HBM)] * 3,
-        out_specs=pl.BlockSpec(memory_space=pl.ANY),
+        layer_kernel,
+        out_shape=(
+            jax.ShapeDtypeStruct((ROWS, D), jnp.float32),
+            jax.ShapeDtypeStruct((SLOTS, ROWS), bf16),
+            jax.ShapeDtypeStruct((SLOTS, ROWS), bf16),
+            jax.ShapeDtypeStruct(half, bf16),
+        ),
+        in_specs=[vmem] * 3 + [hbm] * 12,
+        out_specs=(vmem,) * 3 + (hbm,),
         scratch_shapes=[
-            pltpu.VMEM((4, D, TILE), jnp.bfloat16),
-            pltpu.VMEM((4, D, TILE), jnp.bfloat16),
-            pltpu.VMEM((4, TILE, D), jnp.bfloat16),
-            pltpu.VMEM((count, D), jnp.bfloat16),
-            pltpu.VMEM((4, count, TILE), jnp.bfloat16),
-            pltpu.VMEM((NCOL, CAP, D), jnp.bfloat16),
-            pltpu.VMEM(third, jnp.bfloat16),
-            pltpu.VMEM(third, jnp.bfloat16),
-            pltpu.VMEM(half, jnp.bfloat16),
-            pltpu.SemaphoreType.DMA((3,)),
-            pltpu.SemaphoreType.DMA((2, 3, GROUPS)),
-            pltpu.SemaphoreType.DMA((2, NCOL)),
-            pltpu.SemaphoreType.DMA((2, NCOL)),
+            pltpu.VMEM((SPAN, 256), bf16),
+            pltpu.VMEM((2 * HD, SPAN), bf16),
+            pltpu.VMEM((1024, D), bf16),
+            pltpu.VMEM((ROWS, D), bf16),
+            pltpu.VMEM((1, D), jnp.float32),
+            pltpu.VMEM((1, D), jnp.float32),
+            pltpu.VMEM((TOPK, ROWS), jnp.int32),
+            pltpu.VMEM((TOPK, ROWS), jnp.float32),
+            pltpu.VMEM((5, W, 128), bf16),
+            pltpu.VMEM((5, 1, 128), jnp.float32),
+            pltpu.VMEM((NT, ROWS, 256), bf16),
+            pltpu.VMEM((NT, ROWS, 256), bf16),
+            pltpu.VMEM((ROWS, D), bf16),
+            pltpu.VMEM((SLOTS, ROWS), bf16),
+            pltpu.VMEM(half, bf16),
+            pltpu.VMEM((4, D, TILE), bf16),
+            pltpu.VMEM((4, D, TILE), bf16),
+            pltpu.VMEM((4, TILE, D), bf16),
+            pltpu.VMEM((4, NCOL, CAP, D), bf16),
+            pltpu.VMEM((NCOL, CAP, D), bf16),
+            pltpu.VMEM((count, D), bf16),
+            pltpu.VMEM((4, count, TILE), bf16),
+            pltpu.VMEM((NCOL, CAP, D), bf16),
+            pltpu.VMEM(third, bf16),
+            pltpu.VMEM(third, bf16),
+            pltpu.VMEM(half, bf16),
+            dma((9,)),
+            dma((2, 4)),
+            dma((2, 4)),
+            dma((2, 3, 2)),
+            dma((2, 3, 2)),
+            dma((2, NCOL)),
+            dma((2, NCOL)),
+            dma((2,)),
+            dma((2, 3, len(SPLIT))),
+            dma((2, 3, len(SPLIT))),
+            dma((2, NCOL)),
+            dma((2, NCOL)),
         ],
         compiler_params=pltpu.CompilerParams(
-            collective_id=1, has_side_effects=True, vmem_limit_bytes=58 << 20
+            collective_id=0, has_side_effects=True, vmem_limit_bytes=60 << 20
         ),
         cost_estimate=pl.CostEstimate(
-            flops=13_000_000_000, bytes_accessed=150_000_000, transcendentals=0
+            flops=14_000_000_000, bytes_accessed=300_000_000, transcendentals=0
         ),
-    )(rows_in, gate, up, down)
+    )(*arrays)
 
 
 def rms_scale(vector):
@@ -666,7 +611,7 @@
         ],
         axis=0,
     )
-    after_mix, outgoing, coarse, fine, gate, up, down = attend(
+    after_mix, coarse, fine, returned = layer(
         cosine,
         sine,
         aux,
@@ -683,8 +628,7 @@
         up_weight[0],
         down_weight[0],
     )
-    rows_in = dispatch(outgoing.reshape(2, NCOL, CAP, D))
-    returned = expert_outputs(rows_in, gate, up, down).reshape(SLOTS, D)
+    returned = returned.reshape(SLOTS, D)
     contract = (((0,), (0,)), ((), ()))
     expert_mix = lax.dot_general(
         coarse, returned, contract, preferred_element_type=jnp.float32

time: 201 us -> 168 us (0.84)
  Pallas kernels: 192 us -> 160 us
    pallas_call x3 -> x1, Pallas kernels: 192 us -> 160 us  [layer(): pl.pallas_call(layer_kernel, out_shape=(jax.ShapeDtypeStruct((ROWS, D), j...]
where the time goes in v2:
time: 168 us
  Pallas kernels  160 us (95%)
  other arithmetic  3.79 us (2%)
  matrix products  2.89 us (2%)
    pallas_call x1, Pallas kernels, layer(): pl.pallas_call(layer_kernel, out_shape=(jax.ShapeDtypeStruct((ROWS, D), j...  160 us

profile of v2, /device:TPU:1, one launch (start us, length us, event | category | flops | bytes accessed | tf_op | source)
XLA Modules:
  0.0 168.2 jit_solution(2324345084649673020)
XLA Ops:
  0.0 0.7 pad.2.clone
  0.7 0.1 pad.1.clone
  0.8 0.7 convert_bitcast_fusion
  1.5 0.7 maximum_maximum_fusion.aux_ref
  2.2 1.5 fusion
  3.7 160.1 %shard_map.145 = (f32[96,2048]{1,0:T(8,128)}, bf16[512,96]{1,0:T(8,128)(2,1)}, bf16[512,96]{1,0:T(8,128)(2,1)}, bf16[2,32,8,2048]{3,2,1,0:T(8,128)(2,1)}) custom-call(f32[384,128]{1,0:T(8,128)} %get-tuple-element.14.cos_ref, f32[384,128]{1,0:T(8,128)} %get-tuple-element.13.sin_ref, f32[8,128]{1,0:T(8,128)} %maximum_maximum_fusion.aux_ref, ...), custom_call_target="tpu_custom_call" | custom-call | flops 14000000000 | bytes 300000000 | tf_op jit(solution)/shard_map/pallas_call | solution.py:519
  163.8 0.0 copy-start
  163.8 0.0 copy-start.2
  163.8 2.3 %fusion.5 = f32[96,2048]{1,0:T(8,128)S(1)} fusion(bf16[512,96]{1,0:T(8,128)(2,1)} %get-tuple-element.10, bf16[512,2048]{1,0:T(8,128)(2,1)} %bitcast.17), kind=kOutput, calls=%fused_computation.17 | convolution fusion | flops 201326592 | bytes 2981888 | tf_op jit(solution)/shard_map/dot_general | solution.py:633
  166.1 0.0 copy-done
  166.1 0.0 copy-done.2
  166.1 0.0 copy-start.1
  166.1 0.0 copy-start.3
  166.1 0.6 multiply_reduce_fusion
  166.7 0.5 copy-done.1
  167.3 0.0 copy-done.3
  167.3 0.9 add_convert_fusion
  (3 shorter events, 0.0 us)
Async XLA Ops:
  163.8 2.3 %copy-start = (bf16[2,32,8,2048]{3,2,1,0:T(8,128)(2,1)S(1)}, bf16[2,32,8,2048]{3,2,1,0:T(8,128)(2,1)}, u32[]{:S(2)}) copy-start(bf16[2,32,8,2048]{3,2,1,0:T(8,128)(2,1)} %get-tuple-element.11) | copy-start | bytes 6291460
  163.8 2.3 %copy-start.2 = (bf16[512,96]{1,0:T(8,128)(2,1)S(1)}, bf16[512,96]{1,0:T(8,128)(2,1)}, u32[]{:S(2)}) copy-start(bf16[512,96]{1,0:T(8,128)(2,1)} %get-tuple-element.12) | copy-start | bytes 294916
  166.1 1.1 copy-start.1
  166.1 1.1 copy-start.3

commit v3 on v2

--- a/solution.py
+++ b/solution.py
@@ -71,7 +71,8 @@
 def layer_kernel(
     cos_ref,
     sin_ref,
-    aux_ref,
+    doc_hbm,
+    sink_hbm,
     q_hbm,
     k_hbm,
     v_hbm,
@@ -96,6 +97,7 @@
     ffn_ref,
     routes_ref,
     logits_ref,
+    sink_ref,
     kv_ext,
     doc_ext,
     attended,
@@ -144,6 +146,10 @@
                 (k_hbm, kv_ref.at[pl.ds(0, HD)]),
                 (v_hbm, kv_ref.at[pl.ds(HD, HD)]),
                 (q_hbm, q_ref),
+                (sink_hbm, sink_ref),
+                (doc_hbm.at[pl.ds(0, W)], doc_ext.at[1, 0]),
+                (doc_hbm.at[pl.ds(W, W)], doc_ext.at[2, 0]),
+                (doc_hbm.at[pl.ds(2 * W, W)], doc_ext.at[3, 0]),
                 (routes_hbm, routes_ref),
                 (logits_hbm, logits_ref),
                 (wo_hbm, wo_buf),
@@ -176,8 +182,7 @@
             )
 
     move(0)
-    move(1)
-    for load in loads[:3]:
+    for load in loads[:7]:
         load.wait()
 
     lane = lax.broadcasted_iota(jnp.int32, (128, 128), 1)
@@ -193,7 +198,6 @@
         pair = kv_ref[:, block * W : block * W + W].astype(jnp.float32).T
         key_turned = turned(pair, cos_ref[rows, :], sin_ref[rows, :])
         kv_ext[block + 1] = jnp.where(left, key_turned, pair).astype(jnp.bfloat16)
-        doc_ext[block + 1] = aux_ref[block : block + 1, :]
     halos = [
         remote(kv_ext.at[1], kv_ext.at[4], halo_sem.at[0, 0], halo_sem.at[1, 0], below),
         remote(kv_ext.at[3], kv_ext.at[0], halo_sem.at[0, 1], halo_sem.at[1, 1], above),
@@ -208,7 +212,7 @@
                 halo.wait_recv()
         rows = pl.ds(block * W, W)
         keys_low, keys_high, vals_low, vals_high, keep = [], [], [], [], []
-        doc_query = jnp.broadcast_to(aux_ref[block : block + 1, :], (128, 128)).T
+        doc_query = jnp.broadcast_to(doc_ext[block + 1].astype(jnp.float32), (128, 128)).T
         for part in range(3):
             pair = kv_ext[block + part].astype(jnp.float32)
             other = pltpu.roll(pair, 64, 1)
@@ -218,7 +222,7 @@
             vals_high.append(jnp.where(left, 0.0, pair).astype(jnp.bfloat16))
             gap = (part - 1) * W + lane - lax.broadcasted_iota(jnp.int32, (128, 128), 0)
             place_of = s * SPAN + (block + part - 1) * W + lane
-            doc_key = doc_ext[block + part]
+            doc_key = doc_ext[block + part].astype(jnp.float32)
             keep.append(
                 (jnp.abs(gap) <= W)
                 & (place_of >= 0)
@@ -232,18 +236,18 @@
             columns = pl.ds(duo * 128, 128)
             query = turned(
                 q_ref[rows, columns].astype(jnp.float32), cos_ref[rows, :], sin_ref[rows, :]
-            ).astype(jnp.bfloat16)
+            ).astype(jnp.bfloat16) * HD ** (-0.5)
             out = jnp.zeros((128, 128), jnp.float32)
             for side in range(2):
                 head = 2 * duo + side
                 scores = lax.dot_general(
                     query, keys_of[side], contract, preferred_element_type=jnp.float32
-                ) * HD ** (-0.5)
+                )
                 exponent = jnp.where(keep, jnp.exp(scores), 0.0)
                 denominator = jnp.sum(exponent, axis=1, keepdims=True) + jnp.exp(
-                    aux_ref[4 + head : 5 + head, 0:1]
+                    jnp.full((1, 1), sink_ref[head], jnp.float32)
                 )
-                probs = (exponent / denominator).astype(jnp.bfloat16)
+                probs = (exponent * (1.0 / denominator)).astype(jnp.bfloat16)
                 out = out + jnp.dot(probs, vals_of[side], preferred_element_type=jnp.float32)
             out = out.astype(jnp.bfloat16)
             for piece in range(4):
@@ -264,8 +268,9 @@
             )
         )
     heads[t] = attended[t]
+    move(1)
     move(2)
-    for load in loads[3:]:
+    for load in loads[7:]:
         load.wait()
 
     expert = routes_ref[...]
@@ -479,7 +484,7 @@
                     )
 
     last = len(SPLIT)
-    for step in range(last + 3):
+    for step in range(last + 2):
         if step < last:
             forward(step)
         if step == 0:
@@ -489,12 +494,11 @@
                 copy.wait_recv()
         if 1 <= step <= last:
             compute(step - 1)
-        if step >= 3:
-            add(step - 3)
         if 1 <= step <= last:
             swap(step - 1)
-        if step >= 3:
-            home(step - 3)
+        if step >= 2:
+            add(step - 2)
+            home(step - 2)
     for (kind, index), copy in arrived.items():
         if index != SELF:
             copy.wait_send()
@@ -524,7 +528,7 @@
             jax.ShapeDtypeStruct((SLOTS, ROWS), bf16),
             jax.ShapeDtypeStruct(half, bf16),
         ),
-        in_specs=[vmem] * 3 + [hbm] * 12,
+        in_specs=[vmem] * 2 + [hbm] * 14,
         out_specs=(vmem,) * 3 + (hbm,),
         scratch_shapes=[
             pltpu.VMEM((SPAN, 256), bf16),
@@ -535,8 +539,9 @@
             pltpu.VMEM((1, D), jnp.float32),
             pltpu.VMEM((TOPK, ROWS), jnp.int32),
             pltpu.VMEM((TOPK, ROWS), jnp.float32),
+            pltpu.SMEM((4,), jnp.float32),
             pltpu.VMEM((5, W, 128), bf16),
-            pltpu.VMEM((5, 1, 128), jnp.float32),
+            pltpu.VMEM((5, 1, 128), jnp.int32),
             pltpu.VMEM((NT, ROWS, 256), bf16),
             pltpu.VMEM((NT, ROWS, 256), bf16),
             pltpu.VMEM((ROWS, D), bf16),
@@ -553,7 +558,7 @@
             pltpu.VMEM(third, bf16),
             pltpu.VMEM(third, bf16),
             pltpu.VMEM(half, bf16),
-            dma((9,)),
+            dma((13,)),
             dma((2, 4)),
             dma((2, 4)),
             dma((2, 3, 2)),
@@ -603,18 +608,11 @@
     angles = positions.astype(jnp.float32)[:, None] * inverse[None, :]
     sign = jnp.where(lanes % HD < half_size, -1.0, 1.0)
     cosine, sine = jnp.cos(angles), jnp.sin(angles) * sign[None, :]
-    aux = jnp.concatenate(
-        [
-            documents.astype(jnp.float32).reshape(SPAN // W, W),
-            jnp.zeros((1, W), jnp.float32),
-            jnp.broadcast_to(sink[:, None], (4, W)),
-        ],
-        axis=0,
-    )
     after_mix, coarse, fine, returned = layer(
         cosine,
         sine,
-        aux,
+        documents,
+        sink,
         queries,
         keys.T,
         values.T,

time: 168 us -> 161 us (0.958)
  Pallas kernels: 160 us -> 155 us
    pallas_call x1, Pallas kernels: 160 us -> 155 us  [layer(): pl.pallas_call(layer_kernel, out_shape=(jax.ShapeDtypeStruct((ROWS, D), j...]
where the time goes in v3:
time: 161 us
  Pallas kernels  155 us (96%)
  matrix products  2.89 us (2%)
  other arithmetic  2.44 us (2%)
    pallas_call x1, Pallas kernels, layer(): pl.pallas_call(layer_kernel, out_shape=(jax.ShapeDtypeStruct((ROWS, D), j...  155 us

profile of v3, /device:TPU:1, one launch (start us, length us, event | category | flops | bytes accessed | tf_op | source)
XLA Modules:
  0.0 160.9 jit_solution(5165553548916497241)
XLA Ops:
  0.0 1.5 fusion
  1.5 155.0 %shard_map.145 = (f32[96,2048]{1,0:T(8,128)}, bf16[512,96]{1,0:T(8,128)(2,1)}, bf16[512,96]{1,0:T(8,128)(2,1)}, bf16[2,32,8,2048]{3,2,1,0:T(8,128)(2,1)}) custom-call(f32[384,128]{1,0:T(8,128)} %get-tuple-element.14.cos_ref, f32[384,128]{1,0:T(8,128)} %get-tuple-element.13.sin_ref, s32[384]{0:T(512)} %doc_hbm.1, f32[4]{0:T(128)} %sink_hbm.1, ...), custom_call_target="tpu_custom_call" | custom-call | flops 14000000000 | bytes 300000000 | tf_op jit(solution)/shard_map/pallas_call | solution.py:523
  156.5 0.0 copy-start
  156.5 0.0 copy-start.2
  156.5 2.3 %fusion.5 = f32[96,2048]{1,0:T(8,128)S(1)} fusion(bf16[512,96]{1,0:T(8,128)(2,1)} %get-tuple-element.10, bf16[512,2048]{1,0:T(8,128)(2,1)} %bitcast.14), kind=kOutput, calls=%fused_computation.15 | convolution fusion | flops 201326592 | bytes 2981888 | tf_op jit(solution)/shard_map/dot_general | solution.py:631
  158.8 0.0 copy-done
  158.8 0.0 copy-done.2
  158.8 0.0 copy-start.1
  158.9 0.0 copy-start.3
  158.9 0.6 multiply_reduce_fusion
  159.5 0.5 copy-done.1
  160.0 0.0 copy-done.3
  160.0 0.9 add_convert_fusion
  (3 shorter events, 0.0 us)
Async XLA Ops:
  156.5 2.3 %copy-start = (bf16[2,32,8,2048]{3,2,1,0:T(8,128)(2,1)S(1)}, bf16[2,32,8,2048]{3,2,1,0:T(8,128)(2,1)}, u32[]{:S(2)}) copy-start(bf16[2,32,8,2048]{3,2,1,0:T(8,128)(2,1)} %get-tuple-element.11) | copy-start | bytes 6291460
  156.5 2.3 %copy-start.2 = (bf16[512,96]{1,0:T(8,128)(2,1)S(1)}, bf16[512,96]{1,0:T(8,128)(2,1)}, u32[]{:S(2)}) copy-start(bf16[512,96]{1,0:T(8,128)(2,1)} %get-tuple-element.12) | copy-start | bytes 294916
  158.8 1.1 copy-start.1
  158.9 1.1 copy-start.3
